TPU v7x, 512 devices: a whole 4x8x8 slice. The times are simulated.
512 devices in a mesh: fs: 64 (over z, y), tp: 8 (over x, core).
Axes of the slice: x: 4, y: 8, z: 8, core: 2. Of those that a mesh axis runs over, the one named last changes fastest.
Arguments:
- tokens: bfloat16 [24576, 2048], P('fs', 'tp'), may hold values from -24 to 24, as said below
- mixer_gain: float32 [2048], replicated, may hold values from 0.1 to 1.9
- w_content: float32 [2048, 1024], P('fs', 'tp'), may hold values from -0.125 to 0.125
- w_spatial: float32 [2048, 1024], P('fs', 'tp'), may hold values from -0.125 to 0.125
- content_scale: float32 [1024], P('tp'), may hold values from 0.5 to 2
- spatial_scale: float32 [1024], P('tp'), may hold values from 0.2 to 3.5, as said below
- spatial_gain: float32 [1024], P('tp'), may hold values from 0.1 to 1.9
- block_mixing: bfloat16 [8, 128, 128], P('tp'), may hold values from -0.5 to 0.5
- block_bias: float32 [8, 128], P('tp'), may hold values from -6 to 6
- w_project: float32 [1024, 2048], P('tp', 'fs'), may hold values from -0.1875 to 0.1875
- project_scale: float32 [2048], P('fs'), may hold values from 0.5 to 2
- channel_gain: float32 [2048], replicated, may hold values from 0.1 to 1.9
- w_up: float32 [2048, 8192], P('fs', 'tp'), may hold values from -0.125 to 0.125
- up_scale: float32 [8192], P('tp'), may hold values from 0.5 to 2
- w_down: float32 [8192, 2048], P('tp', 'fs'), may hold values from -0.0625 to 0.0625
- down_scale: float32 [2048], P('fs'), may hold values from 0.5 to 2
Outputs:
- layer_out: bfloat16 [24576, 2048], P('fs', 'tp')
Inputs may be any that keep to these rules, and one draw needn't show every extreme that they name: `tokens`: activations whose features and rows have differing scales. `spatial_scale`: positive column scales.
All inputs are finite; a program needn't handle non-finite values.
Results may differ from a plain program's by a relative error of at most 0.019.
Values may be sent and summed in bfloat16 or wider, within the bound.
A program may use at most 64 MiB of HBM per device.

v0:
```python
import jax
import jax.numpy as jnp
from jax import lax
from jax.sharding import PartitionSpec as P

EPSILON = 1e-06


def gather_turned(arrays, axis, dims):
    turned = [jnp.moveaxis(a, dim, 0) for a, dim in zip(arrays, dims)]
    both = jnp.concatenate([t.reshape(len(t), -1) for t in turned], axis=1)
    result, at, finished = (lax.all_gather(both, axis, axis=0, tiled=True), 0, [])
    for t, dim in zip(turned, dims):
        section = result[:, at : at + t[0].size].reshape(-1, *t.shape[1:])
        finished.append(jnp.moveaxis(section, 0, dim))
        at += t[0].size
    return tuple(finished)


def in_order(blocks, dim):
    blocks = jnp.moveaxis(blocks, 0, dim)
    dims = blocks.shape
    return blocks.reshape(*dims[:dim], dims[dim] * dims[dim + 1], *dims[dim + 2 :])


def sent_to_all(shard, axis):
    size = lax.axis_size(axis)
    return lax.all_to_all(
        jnp.broadcast_to(shard[None], (size, *shard.shape)), axis, 0, 0, tiled=True
    )


def gathered_copies(shard, axis, dim):
    return in_order(sent_to_all(shard, axis), dim)


def over_copies(shard, axis):
    return sent_to_all(shard, axis).sum(axis=0)


def in_blocks(shard, dim, size):
    before, after = (shard.shape[:dim], shard.shape[dim + 1 :])
    return jnp.moveaxis(shard.reshape(*before, size, -1, *after), dim, 0)


def summed_on_arrival(shard, axis, dim):
    size = lax.axis_size(axis)
    blocks = lax.all_to_all(in_blocks(shard, dim, size), axis, 0, 0, tiled=True)
    return jnp.sum(blocks.astype(jnp.float32), axis=0)


def normalize_rows(token_rows, gain_vector):
    values = token_rows.astype(jnp.float32)
    scaled = values * lax.rsqrt(jnp.mean(values * values, axis=-1, keepdims=True) + EPSILON)
    return (scaled * gain_vector).astype(jnp.bfloat16)


def shards(
    tokens,
    mixer_gain,
    w_content,
    w_spatial,
    content_scale,
    spatial_scale,
    spatial_gain,
    block_mixing,
    block_bias,
    w_project,
    project_scale,
    channel_gain,
    w_up,
    up_scale,
    w_down,
    down_scale,
):
    content_weight = w_content.astype(jnp.bfloat16)
    spatial_weight = w_spatial.astype(jnp.bfloat16)
    project_weight = w_project.astype(jnp.bfloat16)
    up_weight = w_up.astype(jnp.bfloat16)
    down_weight = w_down.astype(jnp.bfloat16)
    project_full, down_full = gather_turned((project_scale, down_scale), "fs", (0, 0))
    gathered_rows = gathered_copies(tokens, "tp", 1)
    normed = normalize_rows(gathered_rows, mixer_gain)
    row_count = gathered_rows.shape[0]
    content_full, spatial_full, project_cols = gather_turned(
        (content_weight, spatial_weight, project_weight), "fs", (0, 0, 1)
    )
    content_linear = jnp.dot(normed, content_full, preferred_element_type=jnp.float32)
    spatial_linear = jnp.dot(normed, spatial_full, preferred_element_type=jnp.float32)
    content = jax.nn.gelu(content_linear * content_scale)
    spatial = jax.nn.gelu(spatial_linear * spatial_scale)
    square_sums = over_copies(jnp.sum(spatial * spatial, axis=1), "tp")
    total_width = spatial.shape[1] * lax.axis_size("tp")
    spatial_norm = (
        spatial * lax.rsqrt(square_sums / total_width + EPSILON)[:, None] * spatial_gain
    ).astype(jnp.bfloat16)
    groups_here = block_mixing.shape[0]
    block_size = block_mixing.shape[1]
    group_width = spatial_norm.shape[1] // groups_here
    causal_mask = jnp.tril(jnp.ones((block_size, block_size), dtype=bool))
    mixing_weights = jnp.where(causal_mask[None, :, :], block_mixing, jnp.zeros_like(block_mixing))
    grouped = spatial_norm.reshape(row_count // block_size, block_size, groups_here, group_width)
    mixed_block = (
        jnp.einsum("gts,nsgc->ntgc", mixing_weights, grouped, preferred_element_type=jnp.float32)
        + block_bias.T[None, :, :, None]
    )
    gated = (content * mixed_block.reshape(row_count, spatial_norm.shape[1])).astype(jnp.bfloat16)
    mixer_terms = jnp.dot(gated, project_cols, preferred_element_type=jnp.float32) * project_full
    mixer_sum = summed_on_arrival(mixer_terms.astype(jnp.bfloat16), "tp", 1)
    middle = (tokens.astype(jnp.float32) + mixer_sum).astype(jnp.bfloat16)
    middle_rows = gathered_copies(middle, "tp", 1)
    channel_normed = normalize_rows(middle_rows, channel_gain)
    up_full, down_cols = gather_turned((up_weight, down_weight), "fs", (0, 1))
    up_linear = jnp.dot(channel_normed, up_full, preferred_element_type=jnp.float32)
    hidden = jnp.square(jax.nn.relu(up_linear * up_scale)).astype(jnp.bfloat16)
    channel_terms = jnp.dot(hidden, down_cols, preferred_element_type=jnp.float32) * down_full
    channel_sum = summed_on_arrival(channel_terms.astype(jnp.bfloat16), "tp", 1)
    return (middle.astype(jnp.float32) + channel_sum).astype(jnp.bfloat16)


def solution(mesh):
    return jax.shard_map(
        shards,
        mesh=mesh,
        in_specs=(
            P("fs", "tp"),
            P(),
            P("fs", "tp"),
            P("fs", "tp"),
            P("tp"),
            P("tp"),
            P("tp"),
            P("tp", None, None),
            P("tp", None),
            P("tp", "fs"),
            P("fs"),
            P(),
            P("fs", "tp"),
            P("tp"),
            P("tp", "fs"),
            P("fs"),
        ),
        out_specs=P("fs", "tp"),
        check_vma=False,
    )
```

profile of v0, /device:TPU:1, one launch (start us, length us, event | category | flops | bytes accessed | tf_op | source)
XLA Modules:
  0.0 238.0 jit_solution(6624533297289008726)
XLA Ops:
  6.5 0.0 all-gather.4.cloned.1.call-start
  6.5 0.7 convert_bitcast_fusion.1
  7.3 0.7 convert_element_type.86
  8.0 0.7 convert_element_type.87
  8.7 0.6 pad_maximum_fusion.1
  9.3 0.0 all-gather.4.cloned.1.call-update
  9.3 0.0 all-gather.6.cloned.1.call-start
  9.4 0.9 convert_element_type.100
  10.3 0.9 convert_bitcast_fusion
  11.2 0.7 pad_maximum_fusion
  11.9 0.0 all-gather.6.cloned.1.call-update
  11.9 1.1 copy.30
  13.0 1.3 broadcast_in_dim.9
  14.3 0.0 copy-start.6
  14.3 0.0 copy-start.7
  14.3 10.5 %all-to-all-start = ((bf16[8,384,256]{1,2,0:T(8,128)(2,1)}), bf16[8,384,256]{1,2,0:T(8,128)(2,1)S(1)}, u32[]{:S(2)}, u32[]{:S(2)}) async-start(bf16[8,384,256]{1,2,0:T(8,128)(2,1)} %broadcast_in_dim.9), calls=%async_computation | async-start | bytes 3145728 | tf_op jit(solution)/shard_map/all_to_all | solution.py:28
  24.7 0.0 copy-start.2
  24.7 0.0 copy-done.6
  24.7 0.0 copy-done.7
  24.8 42.5 %all-gather = f32[64,32,2]{1,2,0:T(2,128)S(1)} all-gather(f32[1,32,2]{1,2,0:T(2,128)S(1)} %maximum_bitcast_fusion), channel_id=1, replica_groups=mesh['fs'=64,'tp'=8] {'fs'}, dimensions={0}, use_global_device_ids=true | all-gather | bytes 16640 | tf_op jit(solution)/shard_map/all_gather | solution.py:12
  67.3 0.1 reshape.91
  67.4 0.0 all-to-all-done
  67.4 0.4 multiply_reduce_fusion.1
  67.8 0.0 copy-done.2
  67.8 0.0 copy-start.9
  67.9 0.4 fusion.7
  68.3 0.0 copy-start.4
  68.3 0.0 copy-start.1
  68.3 0.0 copy-start.5
  68.3 0.0 copy-start.10
  68.3 25.8 %all-gather.4.cloned.1.call-done = bf16[2048,384]{1,0:T(8,128)(2,1)} async-done(((bf16[32,384]{1,0:T(8,128)(2,1)}), bf16[2048,384]{1,0:T(8,128)(2,1)}) %all-gather.4.cloned.1.call-update) | async-done | bytes 1572880 | tf_op jit(solution)/shard_map/all_gather | solution.py:12
  94.1 0.0 copy-done.9
  94.1 1.8 multiply_reduce_fusion.2
  95.8 0.6 broadcast_in_dim.10
  96.5 9.5 %all-to-all-start.1 = ((f32[8,1,384]{2,1,0:T(1,128)}), f32[8,1,384]{2,1,0:T(1,128)S(1)}, u32[]{:S(2)}, u32[]{:S(2)}) async-start(f32[8,1,384]{2,1,0:T(1,128)} %broadcast_in_dim.10), calls=%async_computation.1 | async-start | bytes 24576 | tf_op jit(solution)/shard_map/all_to_all | solution.py:28
  106.0 4.6 %all-to-all-done.1 = f32[8,1,384]{2,1,0:T(1,128)S(1)} async-done(((f32[8,1,384]{2,1,0:T(1,128)}), f32[8,1,384]{2,1,0:T(1,128)S(1)}, u32[]{:S(2)}, u32[]{:S(2)}) %all-to-all-start.1) | async-done | bytes 12320 | tf_op jit(solution)/shard_map/all_to_all | solution.py:28
  110.7 0.0 copy-done.4
  110.7 0.1 multiply_convert_fusion.3
  110.8 0.0 copy-done.1
  110.8 0.0 copy-done.5
  110.8 0.2 fusion.14
  111.0 0.0 copy-done.10
  111.0 3.0 %multiply_convert_fusion.1 = bf16[384,2048]{1,0:T(8,128)(2,1)S(1)} fusion(f32[2048]{0:T(1024)S(1)} %bitcast.66, bf16[2048,384]{1,0:T(8,128)(2,1)} %all-gather.4.cloned.1.call-done, f32[384,128]{1,0:T(8,128)S(1)} %bitcast.64, bf16[384,2048]{0,1:T(8,128)(2,1)S(1)} %fusion.7, f32[128]{0:T(128)S(1)} %copy-done.10), kind=kOutput, calls=%fused_computation.14 | convolution fusion | flops 404766720 | bytes 4399616 | tf_op jit(solution)/shard_map/dot_general | solution.py:108
  114.0 0.1 copy.42
  114.2 23.7 %all_to_all.26 = bf16[8,384,256]{2,1,0:T(8,128)(2,1)S(1)} all-to-all(bf16[8,384,256]{2,1,0:T(8,128)(2,1)S(1)} %bitcast.59), channel_id=1, replica_groups=mesh['fs'=64,'tp'=8] {'tp'}, dimensions={0} | all-to-all | bytes 3145728 | tf_op jit(solution)/shard_map/all_to_all | solution.py:48
  137.8 0.0 copy-start
  137.8 0.2 convert_reduce_fusion.1
  138.1 0.7 copy-done
  138.8 0.2 copy.34
  139.0 0.1 broadcast_in_dim.12
  139.1 24.1 %all_to_all.27 = bf16[8,384,256]{1,2,0:T(8,128)(2,1)S(1)} all-to-all(bf16[8,384,256]{1,2,0:T(8,128)(2,1)S(1)} %broadcast_in_dim.12), channel_id=1, replica_groups=mesh['fs'=64,'tp'=8] {'tp'}, dimensions={0} | all-to-all | bytes 3145728 | tf_op jit(solution)/shard_map/all_to_all | solution.py:28
  163.2 0.0 copy-start.3
  163.2 0.4 multiply_reduce_fusion
  163.6 0.3 copy-done.3
  163.9 0.0 copy-start.8
  163.9 0.4 fusion.5
  164.3 33.2 %all-gather.6.cloned.1.call-done = bf16[2048,2048]{1,0:T(8,128)(2,1)} async-done(((bf16[32,2048]{1,0:T(8,128)(2,1)}), bf16[2048,2048]{1,0:T(8,128)(2,1)}) %all-gather.6.cloned.1.call-update) | async-done | bytes 8388624 | tf_op jit(solution)/shard_map/all_gather | solution.py:12
  197.6 0.0 copy-done.8
  197.6 6.9 %multiply_convert_fusion = bf16[384,2048]{1,0:T(8,128)(2,1)S(1)} fusion(bf16[2048,2048]{1,0:T(8,128)(2,1)} %all-gather.6.cloned.1.call-done, f32[2048]{0:T(1024)S(1)} %bitcast.65, bf16[384,2048]{0,1:T(8,128)(2,1)S(1)} %fusion.5, f32[1024]{0:T(1024)S(1)} %copy-done.8), kind=kOutput, calls=%fused_computation.11 | convolution fusion | flops 3224371200 | bytes 11546624 | tf_op jit(solution)/shard_map/dot_general | solution.py:116
  204.5 0.1 copy.41
  204.6 25.5 %all_to_all.28 = bf16[8,384,256]{2,1,0:T(8,128)(2,1)S(1)} all-to-all(bf16[8,384,256]{2,1,0:T(8,128)(2,1)S(1)} %bitcast.60), channel_id=1, replica_groups=mesh['fs'=64,'tp'=8] {'tp'}, dimensions={0} | all-to-all | bytes 3145728 | tf_op jit(solution)/shard_map/all_to_all | solution.py:48
  230.2 0.2 convert_reduce_fusion
  230.4 0.7 add_convert_fusion
  (8 shorter events, 0.1 us)
Async XLA Ops:
  6.5 87.6 %all-gather.4.cloned.1.call-start = ((), (), s32[]{:S(2)}) async-start(), calls=%async_computation.5 | async-start | bytes 1597440 | tf_op jit(solution)/shard_map/all_gather | solution.py:12
  9.3 188.2 %all-gather.6.cloned.1.call-start = ((), (), s32[]{:S(2)}) async-start(), calls=%async_computation.6 | async-start | bytes 8519680 | tf_op jit(solution)/shard_map/all_gather | solution.py:12
  14.3 10.5 %copy-start.6 = (f32[32]{0:T(128)S(1)}, f32[32]{0:T(128)}, u32[]{:S(2)}) copy-start(f32[32]{0:T(128)} %param.31) | copy-start | bytes 388
  14.3 10.5 %copy-start.7 = (f32[32]{0:T(128)S(1)}, f32[32]{0:T(128)}, u32[]{:S(2)}) copy-start(f32[32]{0:T(128)} %param.26) | copy-start | bytes 388
  14.3 53.1 %all-to-all-start = ((bf16[8,384,256]{1,2,0:T(8,128)(2,1)}), bf16[8,384,256]{1,2,0:T(8,128)(2,1)S(1)}, u32[]{:S(2)}, u32[]{:S(2)}) async-start(bf16[8,384,256]{1,2,0:T(8,128)(2,1)} %broadcast_in_dim.9), calls=%async_computation | async-start | bytes 3145728 | tf_op jit(solution)/shard_map/all_to_all | solution.py:28
  24.7 43.1 %copy-start.2 = (f32[2048]{0:T(1024)S(1)}, f32[2048]{0:T(1024)}, u32[]{:S(2)}) copy-start(f32[2048]{0:T(1024)} %param.17) | copy-start | bytes 24580
  67.8 26.2 %copy-start.9 = (f32[128]{0:T(128)S(1)}, f32[128]{0:T(128)}, u32[]{:S(2)}) copy-start(f32[128]{0:T(128)} %param.21) | copy-start | bytes 1540
  68.3 42.4 %copy-start.4 = (f32[128]{0:T(128)S(1)}, f32[128]{0:T(128)}, u32[]{:S(2)}) copy-start(f32[128]{0:T(128)} %param.22) | copy-start | bytes 1540
  68.3 42.5 %copy-start.1 = (bf16[1,128,128]{2,1,0:T(8,128)(2,1)S(1)}, bf16[1,128,128]{2,1,0:T(8,128)(2,1)}, u32[]{:S(2)}) copy-start(bf16[1,128,128]{2,1,0:T(8,128)(2,1)} %param.23) | copy-start | bytes 98308
  68.3 42.5 %copy-start.5 = (f32[1,128]{1,0:T(1,128)S(1)}, f32[1,128]{1,0:T(1,128)}, u32[]{:S(2)}) copy-start(f32[1,128]{1,0:T(1,128)} %param.24) | copy-start | bytes 1540
  68.3 42.7 %copy-start.10 = (f32[128]{0:T(128)S(1)}, f32[128]{0:T(128)}, u32[]{:S(2)}) copy-start(f32[128]{0:T(128)} %param.20) | copy-start | bytes 1540
  96.5 14.2 %all-to-all-start.1 = ((f32[8,1,384]{2,1,0:T(1,128)}), f32[8,1,384]{2,1,0:T(1,128)S(1)}, u32[]{:S(2)}, u32[]{:S(2)}) async-start(f32[8,1,384]{2,1,0:T(1,128)} %broadcast_in_dim.10), calls=%async_computation.1 | async-start | bytes 24576 | tf_op jit(solution)/shard_map/all_to_all | solution.py:28
  137.8 0.9 copy-start
  163.2 0.7 copy-start.3
  163.9 33.7 %copy-start.8 = (f32[1024]{0:T(1024)S(1)}, f32[1024]{0:T(1024)}, u32[]{:S(2)}) copy-start(f32[1024]{0:T(1024)} %param.29) | copy-start | bytes 12292
Sparse Core Ops, SparseCore 0:
  10.3 83.7 all-gather.3
  97.1 100.3 all-gather.5
where the time goes:
time: 239 us; the launch traced here: 238 us
  blocking collectives  116 us (49%)
  waiting for transfers between devices  63.6 us (27%)
  starting transfers between devices  20 us (8%)
  between operations  13.6 us (6%)
  matrix products  11.9 us (5%)
  other arithmetic  8.33 us (3%)
  local copies, waits for them, and re-layouts  4.63 us (2%)
    all_gather x2, waiting for transfers between devices, gather_turned(): lax.all_gather(both, axis, axis=0, tiled=True)  59 us
    all_to_all x2, blocking collectives, summed_on_arrival(): blocks = lax.all_to_all(in_blocks(shard, dim, size), axis, 0, 0, tiled=True)  49.2 us
    all_gather x1, blocking collectives, gather_turned(): lax.all_gather(both, axis, axis=0, tiled=True)  42.5 us
    all_to_all x1, blocking collectives, sent_to_all(): lax.all_to_all(jnp.broadcast_to(shard[None], (size, *shard.shape)), axis,...  24.1 us
    all_to_all x2, starting transfers between devices, sent_to_all(): lax.all_to_all(jnp.broadcast_to(shard[None], (size, *shard.shape)), axis,...  20 us
    dot_general x1, matrix products, shards(): jnp.dot(hidden, down_cols, preferred_element_type=jnp.float32) * down_full  6.94 us
  transfers between devices with their start and end apart: 4, of which 3 were waited for; matrix products, arithmetic and copies ran while one was open for 5% of the time, Pallas kernels for 0%

commit v1 on v0

v1 whole, which is shorter than its diff:
```python
import jax
import jax.numpy as jnp
from jax import lax
from jax.experimental import pallas as pl
from jax.experimental.pallas import tpu as pltpu
from jax.sharding import PartitionSpec as P

EPSILON = 1e-06
MESH = pl.DeviceIdType.MESH
F32 = jnp.float32
BF16 = jnp.bfloat16

RING = 8
HOPS = RING // 2
CHIPS_X = 4
N_TP = 2 * CHIPS_X
SLICE = 32
BLOCK = 128
WIDTHS = (384, 256, 256, 512, 512, 512)


def nt_dot(left, right):
    return lax.dot_general(left, right, (((1,), (1,)), ((), ())), preferred_element_type=F32)


def layer_kernel(
    tokens_ref, mixer_gain_ref, w_content_ref, w_spatial_ref, content_scale_ref, spatial_scale_ref,
    spatial_gain_ref, mixing_ref, bias_ref, w_project_ref, project_scale_ref, channel_gain_ref,
    w_up_ref, up_scale_ref, w_down_ref, down_scale_ref,
    out_ref,
    w0, w1, w2, w3, w4, w5, tok1, tok2, normed, squares, hidden, acc,
    sib_out, sib_in, ring_out, far_in, near_in,
    w_send, w_recv, ag_send, ag_recv, rs_send, rs_recv, sq_send, sq_recv,
):
    chunks = (w0, w1, w2, w3, w4, w5)
    fs, tp = lax.axis_index("fs"), lax.axis_index("tp")
    z, y = fs // RING, fs % RING
    x, core = tp // 2, tp % 2
    p = jnp.where(core == 0, y, z)
    q = jnp.where(core == 0, z, y)

    def fs_of(pp, qq):
        return jnp.where(core == 0, qq * RING + pp, pp * RING + qq)

    def tp_of(dx, other):
        c = (1 - core) if other else core
        return 2 * ((x + dx + CHIPS_X) % CHIPS_X) + c

    first_next = (fs_of((p + 1) % RING, q), fs_of((p + RING - 1) % RING, q))
    second_next = (fs_of(p, (q + 1) % RING), fs_of(p, (q + RING - 1) % RING))

    def remote(src, dst, ss, rs, to_fs, to_tp):
        return pltpu.make_async_remote_copy(
            src_ref=src, dst_ref=dst, send_sem=ss, recv_sem=rs,
            device_id=(to_fs, to_tp), device_id_type=MESH,
        )

    eye = (
        lax.broadcasted_iota(jnp.int32, (SLICE, SLICE), 0)
        == lax.broadcasted_iota(jnp.int32, (SLICE, SLICE), 1)
    ).astype(F32).astype(BF16)

    def turned(w, scale):
        scaled = (w.astype(BF16).astype(F32) * scale).astype(BF16)
        return nt_dot(eye, scaled).astype(BF16)

    w0[q, p, :, 0:128] = w_content_ref[...].astype(BF16)
    w0[q, p, :, 128:256] = w_spatial_ref[...].astype(BF16)
    w0[q, p, :, 256:384] = turned(w_project_ref[...], project_scale_ref[...])
    w1[q, p] = w_up_ref[:, 0:256].astype(BF16)
    w2[q, p] = w_up_ref[:, 256:512].astype(BF16)
    w3[q, p] = w_up_ref[:, 512:1024].astype(BF16)
    w4[q, p] = turned(w_down_ref[0:512], down_scale_ref[...])
    w5[q, p] = turned(w_down_ref[512:1024], down_scale_ref[...])
    tok1[tp] = tokens_ref[...]

    barrier = pltpu.get_barrier_semaphore()
    for to in first_next + second_next:
        pl.semaphore_signal(barrier, inc=1, device_id=(to, tp), device_id_type=MESH)
    for d in range(1, N_TP):
        pl.semaphore_signal(barrier, inc=1, device_id=(fs, (tp + d) % N_TP), device_id_type=MESH)
    pl.semaphore_wait(barrier, 4 + N_TP - 1)

    def weight_copy(ci, phase, way, step, arriving=False):
        shift = step + (1 if arriving else 0)
        if way == 0:
            shift = -shift
        sems = (w_send.at[ci, phase, way, step], w_recv.at[ci, phase, way, step])
        if phase == 0:
            ref = chunks[ci].at[q, (p + shift + RING) % RING]
            if step == HOPS - 1:
                ref = ref.at[pl.ds(way * (SLICE // 2), SLICE // 2)]
            return remote(ref, ref, *sems, first_next[way], tp)
        ref = chunks[ci].at[(q + shift + RING) % RING]
        if step == HOPS - 1:
            ref = ref.at[pl.ds(way * (RING // 2), RING // 2)]
        return remote(ref, ref, *sems, second_next[way], tp)

    def send(ci, phase, step):
        for way in range(2):
            weight_copy(ci, phase, way, step).start()

    def arrived(ci, phase, step):
        for way in range(2):
            weight_copy(ci, phase, way, step, arriving=True).wait_recv()

    def forward(ci, phase, step):
        for way in range(2):
            weight_copy(ci, phase, way, step - 1, arriving=True).wait_recv()
            weight_copy(ci, phase, way, step).start()

    def second_start(ci):
        arrived(ci, 0, HOPS - 1)
        send(ci, 1, 0)

    half = tokens_ref.shape[0] // 2

    class Gather:
        def __init__(self, buf, n):
            self.buf, self.n = buf, n

        def copy(self, k, arriving=False):
            dx = (0, -1, 1, 2, 0, 0, -1, 1)[k]
            if arriving and k >= 4:
                dx = (-1, 1, -2, 2)[k - 4]
            ref = self.buf.at[tp_of(dx, arriving and k < 4)]
            if k >= 6:
                ref = ref.at[pl.ds((k - 6) * half, half)]
            to = tp_of(0, True) if k < 4 else tp_of((1, -1)[k % 2], False)
            return remote(ref, ref, ag_send.at[self.n, k], ag_recv.at[self.n, k], fs, to)

        def begin(self):
            for k in (4, 5, 0):
                self.copy(k).start()

        def pass_on(self):
            for k in range(2):
                self.copy(4 + k, True).wait_recv()
                self.copy(6 + k).start()
                self.copy(1 + k).start()

        def far(self):
            for k in range(2):
                self.copy(6 + k, True).wait_recv()
            self.copy(3).start()

        def finish(self):
            for k in range(4):
                self.copy(k, True).wait_recv()

        def drain(self):
            for k in range(8):
                self.copy(k).wait_send()

    class Scatter:
        order = (2, 1, -1, 0)

        def __init__(self, n):
            self.n = n

        def sems(self, k):
            return rs_send.at[self.n, k], rs_recv.at[self.n, k]

        def across(self, k):
            return remote(sib_out.at[self.n, k], sib_in.at[self.n, k], *self.sems(k), fs, tp_of(0, True))

        def far(self, way):
            rows = pl.ds(way * half, half)
            return remote(ring_out.at[self.n, 0, rows], far_in.at[self.n, way], *self.sems(4 + way),
                          fs, tp_of((1, -1)[way], False))

        def near(self, way, part):
            rows = pl.ds(part * half, half)
            return remote(ring_out.at[self.n, 1 + way, rows], near_in.at[self.n, way, rows],
                          *self.sems(6 + 2 * way + part), fs, tp_of((1, -1)[way], False))

        def begin(self, block_of):
            for k, dx in enumerate(self.order):
                sib_out[self.n, k] = block_of(k, dx, True).astype(BF16)
                self.across(k).start()
                if k > 0:
                    self.own(block_of, k - 1)
            self.own(block_of, 3)

        def own(self, block_of, k):
            n = self.n
            value = block_of(k, self.order[k], False)
            self.across(k).wait_recv()
            value = value + sib_in[n, k].astype(F32)
            if k == 0:
                ring_out[n, 0] = value.astype(BF16)
                self.far(0).start()
                self.far(1).start()
            else:
                acc[k - 1] = value
                if k < 3:
                    way = k - 1
                    part = 1 - way
                    ring_out[n, k, part * half:(part + 1) * half] = (
                        value[part * half:(part + 1) * half].astype(BF16))
                    self.near(way, part).start()

        def combine(self):
            n = self.n
            for way in range(2):
                self.far(way).wait_recv()
                rows = slice(way * half, (way + 1) * half)
                ring_out[n, 1 + way, rows] = (acc[way, rows] + far_in[n, way].astype(F32)).astype(BF16)
                self.near(way, way).start()

        def finish(self):
            for way in range(2):
                for part in range(2):
                    self.near(way, part).wait_recv()
            n = self.n
            return acc[2] + near_in[n, 0].astype(F32) + near_in[n, 1].astype(F32)

        def drain(self):
            for k in range(4):
                self.across(k).wait_send()
            for way in range(2):
                self.far(way).wait_send()
                for part in range(2):
                    self.near(way, part).wait_send()

    width = tokens_ref.shape[1]

    def normalize(buf, gain_ref):
        total = None
        for t in range(N_TP):
            v = buf[t].astype(F32)
            s = jnp.sum(v * v, axis=1, keepdims=True)
            total = s if total is None else total + s
        r = lax.rsqrt(total / (N_TP * width) + EPSILON)
        for t in range(N_TP):
            cols = slice(t * width, (t + 1) * width)
            normed[:, cols] = (buf[t].astype(F32) * r * gain_ref[:, cols]).astype(BF16)

    def weight_rows(ref, zz, cols):
        pieces = []
        for j in range(RING):
            pieces.append(ref[jnp.where(core == 0, zz, j), jnp.where(core == 0, j, zz), :, cols])
        return jnp.concatenate(pieces, axis=0)

    def all_rows(ref, cols):
        return jnp.concatenate([weight_rows(ref, zz, cols) for zz in range(RING)], axis=0)

    gather1, gather2 = Gather(tok1, 0), Gather(tok2, 1)
    scatter1, scatter2 = Scatter(0), Scatter(1)
    every = range(len(chunks))

    send(0, 0, 0)
    gather1.begin()
    for ci in every[1:]:
        send(ci, 0, 0)
    for step in range(1, HOPS):
        for ci in every:
            forward(ci, 0, step)
        if step == HOPS - 2:
            gather1.pass_on()
    second_start(0)
    second_start(1)
    gather1.far()
    gather1.finish()
    normalize(tok1, mixer_gain_ref)
    forward(0, 1, 1)
    forward(1, 1, 1)
    second_start(2)
    forward(0, 1, 2)
    forward(1, 1, 2)
    second_start(3)
    forward(0, 1, 3)
    forward(1, 1, 3)
    arrived(0, 1, 3)

    linear = jnp.dot(normed[...], all_rows(w0, slice(0, 256)), preferred_element_type=F32)
    spatial = jax.nn.gelu(linear[:, 128:256] * spatial_scale_ref[...])
    sq = spatial * spatial
    sq_high = sq.astype(BF16)
    sq_low = (sq - sq_high.astype(F32)).astype(BF16)
    ones = jnp.ones((8, 128), BF16)
    squares[tp] = nt_dot(ones, sq_high) + nt_dot(ones, sq_low)

    def square_copy(d, arriving=False):
        ref = squares.at[(tp + N_TP - d) % N_TP] if arriving else squares.at[tp]
        return remote(ref, ref, sq_send.at[d - 1], sq_recv.at[d - 1], fs, (tp + d) % N_TP)

    for d in range(1, N_TP):
        square_copy(d).start()
    content = jax.nn.gelu(linear[:, 0:128] * content_scale_ref[...])
    gained = (spatial * spatial_gain_ref[...]).astype(BF16)
    causal = (
        lax.broadcasted_iota(jnp.int32, (BLOCK, BLOCK), 1)
        <= lax.broadcasted_iota(jnp.int32, (BLOCK, BLOCK), 0)
    )
    mixing = jnp.where(causal, mixing_ref[0].astype(F32), 0.0)
    bias = jnp.transpose(jnp.broadcast_to(bias_ref[...], (BLOCK, BLOCK)))
    forward(2, 1, 1)
    forward(3, 1, 1)
    arrived(1, 1, 3)
    for d in range(1, N_TP):
        square_copy(d, True).wait_recv()
    total_sq = squares[0]
    for t in range(1, N_TP):
        total_sq = total_sq + squares[t]
    row_scale = lax.rsqrt(total_sq[0:1] / (N_TP * 128) + EPSILON)
    gated_blocks = []
    for b in range(tokens_ref.shape[0] // BLOCK):
        rows = slice(b * BLOCK, (b + 1) * BLOCK)
        scaled = (mixing * row_scale[:, rows]).astype(BF16)
        mixed = jnp.dot(scaled, gained[rows], preferred_element_type=F32) + bias
        gated_blocks.append((content[rows] * mixed).astype(BF16))
    gated = jnp.concatenate(gated_blocks, axis=0)

    def project_block(k, dx, other):
        return nt_dot(gated, weight_rows(w0, tp_of(dx, other), slice(256, 384)))

    scatter1.begin(project_block)
    forward(2, 1, 2)
    forward(3, 1, 2)
    second_start(4)
    scatter1.combine()
    forward(2, 1, 3)
    forward(3, 1, 3)
    second_start(5)
    middle = tokens_ref[...].astype(F32) + scatter1.finish()
    tok2[tp] = middle.astype(BF16)
    gather2.begin()
    arrived(2, 1, 3)
    arrived(3, 1, 3)
    gather2.pass_on()
    forward(4, 1, 1)
    gather2.far()
    gather2.finish()
    forward(5, 1, 1)
    normalize(tok2, channel_gain_ref)

    at = 0
    for ref in (w1, w2, w3):
        for low in range(0, ref.shape[3], 256):
            up = jnp.dot(normed[...], all_rows(ref, slice(low, low + 256)), preferred_element_type=F32)
            up = jnp.maximum(up * up_scale_ref[:, at:at + 256], 0.0)
            hidden[:, at:at + 256] = (up * up).astype(BF16)
            at += 256
    forward(4, 1, 2)
    forward(5, 1, 2)
    forward(4, 1, 3)
    forward(5, 1, 3)
    arrived(4, 1, 3)

    slots = [(k, other) for k in range(4) for other in (True, False)]
    for i, (k, other) in enumerate(slots):
        zz = tp_of(Scatter.order[k], other)
        acc[3 + i] = nt_dot(hidden[:, 0:512], weight_rows(w4, zz, slice(0, 512)))
    arrived(5, 1, 3)

    def down_block(k, dx, other):
        return acc[3 + 2 * k + (0 if other else 1)] + nt_dot(
            hidden[:, 512:1024], weight_rows(w5, tp_of(dx, other), slice(0, 512)))

    scatter2.begin(down_block)
    scatter2.combine()
    out_ref[...] = (tok2[tp].astype(F32) + scatter2.finish()).astype(BF16)

    for ci in every:
        for phase in range(2):
            for way in range(2):
                for step in range(HOPS):
                    weight_copy(ci, phase, way, step).wait_send()
    gather1.drain()
    gather2.drain()
    scatter1.drain()
    scatter2.drain()
    for d in range(1, N_TP):
        square_copy(d).wait_send()


def shards(
    tokens, mixer_gain, w_content, w_spatial, content_scale, spatial_scale, spatial_gain, block_mixing,
    block_bias, w_project, project_scale, channel_gain, w_up, up_scale, w_down, down_scale,
):
    rows, width = tokens.shape
    row = lambda v: v.reshape(1, -1)
    chunk = lambda n: pltpu.VMEM((RING, RING, SLICE, n), BF16)
    vmem = pl.BlockSpec(memory_space=pltpu.VMEM)
    dma = pltpu.SemaphoreType.DMA
    return pl.pallas_call(
        layer_kernel,
        out_shape=jax.ShapeDtypeStruct((rows, width), BF16),
        in_specs=[vmem] * 16,
        out_specs=vmem,
        scratch_shapes=[chunk(n) for n in WIDTHS] + [
            pltpu.VMEM((N_TP, rows, width), BF16),
            pltpu.VMEM((N_TP, rows, width), BF16),
            pltpu.VMEM((rows, N_TP * width), BF16),
            pltpu.VMEM((N_TP, 8, rows), F32),
            pltpu.VMEM((rows, w_up.shape[1]), BF16),
            pltpu.VMEM((11, rows, width), F32),
            pltpu.VMEM((2, 4, rows, width), BF16),
            pltpu.VMEM((2, 4, rows, width), BF16),
            pltpu.VMEM((2, 3, rows, width), BF16),
            pltpu.VMEM((2, 2, rows // 2, width), BF16),
            pltpu.VMEM((2, 2, rows, width), BF16),
            dma((len(WIDTHS), 2, 2, HOPS)), dma((len(WIDTHS), 2, 2, HOPS)),
            dma((2, 8)), dma((2, 8)), dma((2, 10)), dma((2, 10)), dma((7,)), dma((7,)),
        ],
        compiler_params=pltpu.CompilerParams(
            collective_id=0, has_side_effects=True, vmem_limit_bytes=56 * 1024 * 1024),
        name="layer",
    )(
        tokens, row(mixer_gain), w_content, w_spatial, row(content_scale), row(spatial_scale),
        row(spatial_gain), block_mixing, block_bias, w_project, row(project_scale), row(channel_gain),
        w_up, row(up_scale), w_down, row(down_scale),
    )


def solution(mesh):
    return jax.shard_map(
        shards,
        mesh=mesh,
        in_specs=(
            P("fs", "tp"), P(), P("fs", "tp"), P("fs", "tp"), P("tp"), P("tp"), P("tp"),
            P("tp", None, None), P("tp", None), P("tp", "fs"), P("fs"), P(), P("fs", "tp"), P("tp"),
            P("tp", "fs"), P("fs"),
        ),
        out_specs=P("fs", "tp"),
        check_vma=False,
    )
```

time: 239 us -> 111 us (0.46)
  blocking collectives: 116 us -> 0 us
  Pallas kernels: 0 us -> 106 us
  waiting for transfers between devices: 63.6 us -> 0 us
  starting transfers between devices: 20 us -> 0 us
  between operations: 13.6 us -> 0.01 us
  matrix products: 11.9 us -> 0 us
  other arithmetic: 8.33 us -> 0 us
    pallas_call x0 -> x1, Pallas kernels: none -> 106 us  [shards(): pl.pallas_call(layer_kernel, out_shape=jax.ShapeDtypeStruct((rows, width)...]
    all_to_all x3 -> x0, blocking collectives: 73.3 us -> none  [the longest x2 49.2 us: summed_on_arrival(): blocks = lax.all_to_all(in_blocks(shard, dim, size), axis, 0, 0, tiled=True)]
    all_gather x2 -> x0, waiting for transfers between devices: 59 us -> none  [gather_turned(): lax.all_gather(both, axis, axis=0, tiled=True)]
    all_gather x1 -> x0, blocking collectives: 42.5 us -> none  [gather_turned(): lax.all_gather(both, axis, axis=0, tiled=True)]
    all_to_all x2 -> x0, starting transfers between devices: 20 us -> none  [sent_to_all(): lax.all_to_all(jnp.broadcast_to(shard[None], (size, *shard.shape)), axis,...]
    dot_general x4 -> x0, matrix products: 11.9 us -> none  [the longest x1 6.94 us: shards(): jnp.dot(hidden, down_cols, preferred_element_type=jnp.float32) * down_full]
    all_to_all x2 -> x0, waiting for transfers between devices: 4.62 us -> none  [sent_to_all(): lax.all_to_all(jnp.broadcast_to(shard[None], (size, *shard.shape)), axis,...]
    convert_element_type x8 -> x0, other arithmetic: 4.09 us -> none  [the longest x1 0.92 us: shards(): up_weight = w_up.astype(jnp.bfloat16)]
  transfers between devices with their start and end apart: 4 -> 0, of which waited for: 3 -> 0; matrix products, arithmetic and copies ran while one was open for 5% -> 0% of each run, Pallas kernels for 0% -> 0%
where the time goes in v1:
time: 111 us
  Pallas kernels  106 us (95%)
  local copies, waits for them, and re-layouts  4.96 us (4%)
    pallas_call x1, Pallas kernels, shards(): pl.pallas_call(layer_kernel, out_shape=jax.ShapeDtypeStruct((rows, width)...  106 us
    unnamed x3, local copies, waits for them, and re-layouts  4.96 us

profile of v1, /device:TPU:1, one launch (start us, length us, event | category | flops | bytes accessed | tf_op | source)
XLA Modules:
  0.0 110.7 jit_solution(9049406180456748900)
XLA Ops:
  0.0 1.4 %copy.17.w_project_ref = f32[128,32]{1,0:T(8,128)} copy(f32[128,32]{0,1:T(8,128)} %param.25) | data formatting | bytes 32768 | tf_op args[9]
  1.4 1.9 %copy.18.w_down_ref = f32[1024,32]{1,0:T(8,128)} copy(f32[1024,32]{0,1:T(8,128)} %param.30) | data formatting | bytes 262144 | tf_op args[14]
  3.3 105.7 %layer.1 = bf16[384,256]{1,0:T(8,128)(2,1)} custom-call(bf16[384,256]{1,0:T(8,128)(2,1)} %tokens_ref.1, f32[1,2048]{1,0:T(1,128)} %bitcast.8, f32[32,128]{1,0:T(8,128)} %w_content_ref.1, f32[32,128]{1,0:T(8,128)} %w_spatial_ref.1, f32[1,128]{1,0:T(1,128)} %bitcast.11, f32[1,128]{1,0:T(1,128)} %bitcast.12, f32[1,128]{1,0:T(1,128)} %bitcast.13, ...), custom_call_target="tpu_custom_call" | custom-call | tf_op jit(solution)/shard_map/layer/pallas_call | solution.py:387
  109.1 1.6 %copy.20 = bf16[384,256]{1,0:T(8,128)(2,1)} copy(bf16[384,256]{1,0:T(8,128)(2,1)} %layer.1) | data formatting | bytes 393216

commit v2 on v1

v2 whole, which is shorter than its diff:
```python
import jax
import jax.numpy as jnp
from jax import lax
from jax.experimental import pallas as pl
from jax.experimental.pallas import tpu as pltpu
from jax.sharding import PartitionSpec as P

EPSILON = 1e-06
MESH = pl.DeviceIdType.MESH
F32 = jnp.float32
BF16 = jnp.bfloat16

RING = 8
HOPS = RING // 2
CHIPS_X = 4
N_TP = 2 * CHIPS_X
SLICE = 32
BLOCK = 128
N_INPUTS = 16


def nt_dot(left, right):
    return lax.dot_general(left, right, (((1,), (1,)), ((), ())), preferred_element_type=F32)


def layer_kernel(*refs):
    hbm = refs[:N_INPUTS]
    out_hbm = refs[N_INPUTS]
    inputs = refs[N_INPUTS + 1:2 * N_INPUTS + 1]
    (
        tokens_ref, mixer_gain_ref, w_content_ref, w_spatial_ref, content_scale_ref, spatial_scale_ref,
        spatial_gain_ref, mixing_ref, bias_ref, w_project_ref, project_scale_ref, channel_gain_ref,
        w_up_ref, up_scale_ref, w_down_ref, down_scale_ref,
    ) = inputs
    (
        wa, wb, wu, wd0, wd1, tok1, tok2, normed, squares, hidden, partial, out_ref,
        sib_out1, sib_in1, ring_out1, far_in1, near_in1, acc1,
        sib_out2, sib_in2, ring_out2, far_in2, near_in2, acc2,
        in_sem, out_sem, w1_send, w1_recv, w2_send, w2_recv,
        ag_send, ag_recv, rs_send, rs_recv, sq_send, sq_recv,
    ) = refs[2 * N_INPUTS + 1:]
    fs, tp = lax.axis_index("fs"), lax.axis_index("tp")
    z, y = fs // RING, fs % RING
    x, core = tp // 2, tp % 2
    p = jnp.where(core == 0, y, z)
    q = jnp.where(core == 0, z, y)

    def fs_of(pp, qq):
        return jnp.where(core == 0, qq * RING + pp, pp * RING + qq)

    def tp_of(dx, other):
        c = (1 - core) if other else core
        return 2 * ((x + dx + CHIPS_X) % CHIPS_X) + c

    first_next = (fs_of((p + 1) % RING, q), fs_of((p + RING - 1) % RING, q))
    second_next = (fs_of(p, (q + 1) % RING), fs_of(p, (q + RING - 1) % RING))

    barrier = pltpu.get_barrier_semaphore()
    for to in first_next + second_next:
        pl.semaphore_signal(barrier, inc=1, device_id=(to, tp), device_id_type=MESH)
    for d in range(1, N_TP):
        pl.semaphore_signal(barrier, inc=1, device_id=(fs, (tp + d) % N_TP), device_id_type=MESH)
    fetches = [pltpu.make_async_copy(hbm[i], inputs[i], in_sem.at[i]) for i in range(N_INPUTS)]
    for i in (2, 3, 9, 10, 0, 12, 14, 15, 1, 4, 5, 6, 7, 8, 11, 13):
        fetches[i].start()

    def remote(src, dst, ss, rs, to_fs, to_tp):
        return pltpu.make_async_remote_copy(
            src_ref=src, dst_ref=dst, send_sem=ss, recv_sem=rs,
            device_id=(to_fs, to_tp), device_id_type=MESH,
        )

    eye = (
        lax.broadcasted_iota(jnp.int32, (SLICE, SLICE), 0)
        == lax.broadcasted_iota(jnp.int32, (SLICE, SLICE), 1)
    )

    def scaled(w, scale):
        column = jnp.sum(jnp.where(eye, scale, 0.0), axis=1, keepdims=True)
        return (w.astype(BF16).astype(F32) * column).astype(BF16)

    for i in (2, 3, 9, 10):
        fetches[i].wait()
    wa[q, p, :, 0:128] = w_content_ref[...].astype(BF16)
    wa[q, p, :, 128:256] = w_spatial_ref[...].astype(BF16)
    wb[q, p] = scaled(w_project_ref[...], project_scale_ref[...])
    for i in (0, 12, 14, 15):
        fetches[i].wait()
    tok1[tp] = tokens_ref[...]
    down = scaled(w_down_ref[...], down_scale_ref[...])
    for k in range(2):
        cols = slice(k * 512, (k + 1) * 512)
        wu[k, q, p] = w_up_ref[:, cols].astype(BF16)
        wd0[k, q, p] = down[0:16, cols]
        wd1[k, q, p] = down[16:32, cols]
    pl.semaphore_wait(barrier, 4 + N_TP - 1)

    A, B, U, D0, D1 = range(5)
    first_units = (wa, wb, wu, wd0, wd1)

    def first_copy(u, way, step):
        at = (p + (step if way else -step) + RING) % RING
        if u in (A, B):
            ref = first_units[u].at[q, at]
            if step == HOPS - 1:
                ref = ref.at[pl.ds(way * (SLICE // 2), SLICE // 2)]
        elif step == HOPS - 1:
            ref = first_units[u].at[way, q, at]
        else:
            ref = first_units[u].at[:, q, at]
        return remote(ref, ref, w1_send.at[u], w1_recv.at[u, step], first_next[way], tp)

    def first_send(u, step):
        for way in range(2):
            first_copy(u, way, step).start()

    def first_wait(u, step):
        ref = first_units[u].at[0, 0] if u in (A, B) else first_units[u].at[:, 0, 0]
        if step < HOPS - 1:
            ref = first_units[u].at[0, 0:2] if u in (A, B) else first_units[u].at[:, 0, 0:2]
        remote(ref, ref, w1_send.at[u], w1_recv.at[u, step], first_next[0], tp).wait_recv()

    def first_forward(u, step):
        first_wait(u, step - 1)
        first_send(u, step)

    U0, U1, E0, E1, E2 = 2, 3, 4, 5, 6
    second_units = (wa, wb, wu.at[0], wu.at[1], wd0, wd1.at[0], wd1.at[1])

    def second_copy(u, way, step):
        at = (q + (step if way else -step) + RING) % RING
        ref = second_units[u].at[:, at] if u == E0 else second_units[u].at[at]
        if step == HOPS - 1:
            rows = pl.ds(way * HOPS, HOPS)
            ref = ref.at[:, rows] if u == E0 else ref.at[rows]
        return remote(ref, ref, w2_send.at[u], w2_recv.at[u, step], second_next[way], tp)

    def second_send(u, step=0):
        for way in range(2):
            second_copy(u, way, step).start()

    def second_wait(u, step=HOPS - 1):
        n = 1 if step == HOPS - 1 else 2
        ref = second_units[u].at[:, 0:n] if u == E0 else second_units[u].at[0:n]
        remote(ref, ref, w2_send.at[u], w2_recv.at[u, step], second_next[0], tp).wait_recv()

    def forward(u, step):
        second_wait(u, step - 1)
        second_send(u, step)

    half = tokens_ref.shape[0] // 2

    class Gather:
        def __init__(self, buf, n):
            self.buf, self.n = buf, n

        def copy(self, k, arriving=False):
            dx = (0, -1, 1, 2, 0, 0, -1, 1)[k]
            if arriving and k >= 4:
                dx = (-1, 1, -2, 2)[k - 4]
            ref = self.buf.at[tp_of(dx, arriving and k < 4)]
            if k >= 6:
                ref = ref.at[pl.ds((k - 6) * half, half)]
            to = tp_of(0, True) if k < 4 else tp_of((1, -1)[k % 2], False)
            return remote(ref, ref, ag_send.at[self.n], ag_recv.at[self.n, k], fs, to)

        def begin(self):
            for k in (4, 5, 0):
                self.copy(k).start()

        def pass_on(self):
            for k in range(2):
                self.copy(4 + k, True).wait_recv()
                self.copy(6 + k).start()
                self.copy(1 + k).start()

        def far(self):
            for k in range(2):
                self.copy(6 + k, True).wait_recv()
            self.copy(3).start()

        def finish(self):
            for k in range(4):
                self.copy(k, True).wait_recv()

        def drain(self):
            ref = self.buf.at[0:7]
            remote(ref, ref, ag_send.at[self.n], ag_recv.at[self.n, 0], fs, tp_of(1, False)).wait_send()

    class Scatter:
        order = (2, 1, -1, 0)

        def __init__(self, n, bufs, bytes_ref):
            self.n, self.bytes_ref = n, bytes_ref
            self.sib_out, self.sib_in, self.ring_out, self.far_in, self.near_in, self.acc = bufs

        def copy(self, src, dst, k, to):
            return remote(src, dst, rs_send.at[self.n], rs_recv.at[self.n, k], fs, to)

        def across(self, k):
            return self.copy(self.sib_out.at[k], self.sib_in.at[k], k, tp_of(0, True))

        def far(self, way):
            return self.copy(self.ring_out.at[0, pl.ds(way * half, half)], self.far_in.at[way], 4 + way,
                             tp_of((1, -1)[way], False))

        def near(self, way, part):
            rows = pl.ds(part * half, half)
            return self.copy(self.ring_out.at[1 + way, rows], self.near_in.at[way, rows], 6 + 2 * way + part,
                             tp_of((1, -1)[way], False))

        def begin(self, blocks_of):
            for k, dx in enumerate(self.order):
                across, own = blocks_of(k, dx)
                self.sib_out[k] = across.astype(BF16)
                self.across(k).start()
                self.acc[k] = own
                if k > 0:
                    self.own(k - 1)
            self.own(3)

        def own(self, k):
            self.across(k).wait_recv()
            value = self.acc[k] + self.sib_in[k].astype(F32)
            if k == 0:
                self.ring_out[0] = value.astype(BF16)
                self.far(0).start()
                self.far(1).start()
            else:
                self.acc[k] = value
                if k < 3:
                    part = 2 - k
                    rows = slice(part * half, (part + 1) * half)
                    self.ring_out[k, rows] = value[rows].astype(BF16)
                    self.near(k - 1, part).start()

        def combine(self):
            for way in range(2):
                self.far(way).wait_recv()
                rows = slice(way * half, (way + 1) * half)
                self.ring_out[1 + way, rows] = (
                    self.acc[1 + way, rows] + self.far_in[way].astype(F32)).astype(BF16)
                self.near(way, way).start()

        def finish(self):
            for way in range(2):
                for part in range(2):
                    self.near(way, part).wait_recv()
            return self.acc[3] + self.near_in[0].astype(F32) + self.near_in[1].astype(F32)

        def drain(self):
            remote(self.bytes_ref, self.bytes_ref, rs_send.at[self.n], rs_recv.at[self.n, 0], fs,
                   tp_of(1, False)).wait_send()

    width = tokens_ref.shape[1]

    def normalize(buf, gain_ref):
        total = None
        for t in range(N_TP):
            v = buf[t].astype(F32)
            s = jnp.sum(v * v, axis=1, keepdims=True)
            total = s if total is None else total + s
        r = lax.rsqrt(total / (N_TP * width) + EPSILON)
        for t in range(N_TP):
            cols = slice(t * width, (t + 1) * width)
            normed[:, cols] = (buf[t].astype(F32) * r * gain_ref[:, cols]).astype(BF16)

    def plane_rows(ref, zz, cols):
        return [ref[jnp.where(core == 0, zz, j), jnp.where(core == 0, j, zz), :, cols] for j in range(RING)]

    def all_rows(ref, cols):
        return jnp.concatenate([r for zz in range(RING) for r in plane_rows(ref, zz, cols)], axis=0)

    def set_of(*bufs, low=None):
        return bufs if low is None else tuple(b.at[pl.ds(low * (b.shape[0] // 2), b.shape[0] // 2)] for b in bufs)

    gather1, gather2 = Gather(tok1, 0), Gather(tok2, 1)
    bufs2 = (sib_out2, sib_in2, ring_out2, far_in2, near_in2, acc2)
    scatter1 = Scatter(0, (sib_out1, sib_in1, ring_out1, far_in1, near_in1, acc1), tok1.at[0:7])
    scatter2 = Scatter(1, set_of(*bufs2, low=0), sib_out2.at[0:7])
    scatter3 = Scatter(2, set_of(*bufs2, low=1), sib_out2.at[0:7])

    first_send(A, 0)
    first_send(B, 0)
    gather1.begin()
    first_send(U, 0)
    first_send(D0, 0)
    first_send(D1, 0)
    first_forward(A, 1)
    first_forward(B, 1)
    first_forward(U, 1)
    first_forward(D0, 1)
    first_forward(D1, 1)
    first_forward(A, 2)
    first_forward(B, 2)
    first_forward(U, 2)
    first_forward(D0, 2)
    first_forward(D1, 2)
    first_forward(A, 3)
    first_forward(B, 3)
    gather1.pass_on()
    first_forward(U, 3)
    first_forward(D0, 3)
    first_forward(D1, 3)
    first_wait(A, 3)
    second_send(A)
    first_wait(B, 3)
    second_send(B)
    for i in (1, 4, 5, 6, 7, 8, 11, 13):
        fetches[i].wait()
    gather1.far()
    first_wait(D1, 3)
    second_send(E1)
    gather1.finish()
    normalize(tok1, mixer_gain_ref)
    forward(A, 1)
    forward(B, 1)
    second_send(E2)
    forward(A, 2)
    forward(B, 2)
    first_wait(U, 3)
    first_wait(D0, 3)
    forward(A, 3)
    forward(B, 3)
    second_send(U0)
    second_send(U1)
    second_send(E0)
    second_wait(A)

    linear = jnp.dot(normed[...], all_rows(wa, slice(0, 256)), preferred_element_type=F32)
    spatial = jax.nn.gelu(linear[:, 128:256] * spatial_scale_ref[...])
    sq = spatial * spatial
    sq_high = sq.astype(BF16)
    sq_low = (sq - sq_high.astype(F32)).astype(BF16)
    ones = jnp.ones((8, 128), BF16)
    squares[tp] = nt_dot(ones, sq_high) + nt_dot(ones, sq_low)

    def square_copy(d, arriving=False):
        ref = squares.at[(tp + N_TP - d) % N_TP] if arriving else squares.at[tp]
        return remote(ref, ref, sq_send.at[0], sq_recv.at[d - 1], fs, (tp + d) % N_TP)

    for d in range(1, N_TP):
        square_copy(d).start()
    content = jax.nn.gelu(linear[:, 0:128] * content_scale_ref[...])
    gained = (spatial * spatial_gain_ref[...]).astype(BF16)
    causal = (
        lax.broadcasted_iota(jnp.int32, (BLOCK, BLOCK), 1)
        <= lax.broadcasted_iota(jnp.int32, (BLOCK, BLOCK), 0)
    )
    mixing = jnp.where(causal, mixing_ref[0].astype(F32), 0.0)
    bias = jnp.transpose(jnp.broadcast_to(bias_ref[...], (BLOCK, BLOCK)))
    for d in range(1, N_TP):
        square_copy(d, True).wait_recv()
    total_sq = squares[0]
    for t in range(1, N_TP):
        total_sq = total_sq + squares[t]
    row_scale = lax.rsqrt(total_sq[0:1] / (N_TP * 128) + EPSILON)
    gated_blocks = []
    for b in range(tokens_ref.shape[0] // BLOCK):
        rows = slice(b * BLOCK, (b + 1) * BLOCK)
        mixing_b = (mixing * row_scale[:, rows]).astype(BF16)
        mixed = jnp.dot(mixing_b, gained[rows], preferred_element_type=F32) + bias
        gated_blocks.append((content[rows] * mixed).astype(BF16))
    gated = jnp.concatenate(gated_blocks, axis=0)

    def project_blocks(k, dx):
        return tuple(
            nt_dot(gated, jnp.concatenate(plane_rows(wb, tp_of(dx, other), slice(0, 128)), axis=0))
            for other in (True, False))

    forward(U0, 1)
    second_wait(B)
    scatter1.begin(project_blocks)
    forward(U1, 1)
    scatter1.combine()
    forward(E0, 1)
    forward(U0, 2)
    middle = (tokens_ref[...].astype(F32) + scatter1.finish()).astype(BF16)
    tok2[tp] = middle
    gather2.begin()
    forward(U1, 2)
    forward(E0, 2)
    gather2.pass_on()
    forward(U0, 3)
    forward(E1, 1)
    gather2.far()
    forward(E2, 1)
    gather2.finish()
    forward(U1, 3)
    normalize(tok2, channel_gain_ref)
    forward(E0, 3)

    def up_tiles(k):
        for low in range(0, 512, 256):
            at = k * 512 + low
            up = jnp.dot(normed[...], all_rows(wu.at[k], slice(low, low + 256)), preferred_element_type=F32)
            up = jnp.maximum(up * up_scale_ref[:, at:at + 256], 0.0)
            hidden[:, at:at + 256] = (up * up).astype(BF16)

    second_wait(U0)
    up_tiles(0)
    forward(E1, 2)
    second_wait(U1)
    up_tiles(1)
    forward(E2, 2)

    natural = lax.broadcasted_iota(jnp.int32, (width, width), 0)
    split = lax.broadcasted_iota(jnp.int32, (width, width), 1)
    order = (
        natural == ((split % 128) // 16) * 32 + (split // 128) * 16 + split % 16
    ).astype(F32).astype(BF16)
    middle_split = jnp.dot(middle, order, preferred_element_type=F32)

    def down_pair(ref, k, dx):
        pieces = [r for other in (True, False) for r in plane_rows(ref.at[k], tp_of(dx, other), slice(0, 512))]
        return nt_dot(hidden[:, k * 512:(k + 1) * 512], jnp.concatenate(pieces, axis=0))

    def first_half(k, dx):
        both = down_pair(wd0, 0, dx) + down_pair(wd0, 1, dx)
        return both[:, 0:128], both[:, 128:256]

    def second_half(k, dx):
        both = partial[k] + down_pair(wd1, 1, dx)
        return both[:, 0:128], both[:, 128:256]

    second_wait(E0)
    scatter2.begin(first_half)
    forward(E1, 3)
    forward(E2, 3)
    scatter2.combine()
    second_wait(E1)
    for k, dx in enumerate(Scatter.order):
        partial[k] = down_pair(wd1, 0, dx)
    second_wait(E2)
    scatter3.begin(second_half)
    half0 = (middle_split[:, 0:128] + scatter2.finish()).astype(BF16)
    out0 = nt_dot(half0, order[:, 0:128])
    scatter3.combine()
    half1 = (middle_split[:, 128:256] + scatter3.finish()).astype(BF16)
    out_ref[...] = (out0 + nt_dot(half1, order[:, 128:256])).astype(BF16)
    store = pltpu.make_async_copy(out_ref, out_hbm, out_sem)
    store.start()

    for u in (A, B):
        ref = first_units[u].at[0, 0:7]
        remote(ref, ref, w1_send.at[u], w1_recv.at[u, 0], fs, tp_of(1, False)).wait_send()
    for u in (U, D0, D1):
        ref = first_units[u].at[:, 0, 0:7]
        remote(ref, ref, w1_send.at[u], w1_recv.at[u, 0], fs, tp_of(1, False)).wait_send()
    for u in range(7):
        ref = second_units[u].at[:, 0:7] if u == E0 else second_units[u].at[0:7]
        remote(ref, ref, w2_send.at[u], w2_recv.at[u, 0], fs, tp_of(1, False)).wait_send()
    gather1.drain()
    gather2.drain()
    scatter1.drain()
    scatter2.drain()
    scatter3.drain()
    remote(squares.at[0:7], squares.at[0:7], sq_send.at[0], sq_recv.at[0], fs, tp_of(1, False)).wait_send()
    store.wait()


def shards(
    tokens, mixer_gain, w_content, w_spatial, content_scale, spatial_scale, spatial_gain, block_mixing,
    block_bias, w_project, project_scale, channel_gain, w_up, up_scale, w_down, down_scale,
):
    rows, width = tokens.shape
    row = lambda v: v.reshape(1, -1)
    inputs = (
        tokens, row(mixer_gain), w_content, w_spatial, row(content_scale), row(spatial_scale),
        row(spatial_gain), block_mixing, block_bias, w_project.T, row(project_scale), row(channel_gain),
        w_up, row(up_scale), w_down.T, row(down_scale),
    )
    vmem = pltpu.VMEM
    dma = pltpu.SemaphoreType.DMA
    anywhere = pl.BlockSpec(memory_space=pl.ANY)
    return pl.pallas_call(
        layer_kernel,
        out_shape=jax.ShapeDtypeStruct((rows, width), BF16),
        in_specs=[anywhere] * N_INPUTS,
        out_specs=anywhere,
        scratch_shapes=[vmem(v.shape, v.dtype) for v in inputs] + [
            vmem((RING, RING, SLICE, 256), BF16),
            vmem((RING, RING, SLICE, 128), BF16),
            vmem((2, RING, RING, SLICE, 512), BF16),
            vmem((2, RING, RING, SLICE // 2, 512), BF16),
            vmem((2, RING, RING, SLICE // 2, 512), BF16),
            vmem((N_TP, rows, width), BF16),
            vmem((N_TP, rows, width), BF16),
            vmem((rows, N_TP * width), BF16),
            vmem((N_TP, 8, rows), F32),
            vmem((rows, w_up.shape[1]), BF16),
            vmem((4, rows, width), F32),
            vmem((rows, width), BF16),
            vmem((4, rows, 256), BF16), vmem((4, rows, 256), BF16), vmem((3, rows, 256), BF16),
            vmem((2, rows // 2, 256), BF16), vmem((2, rows, 256), BF16), vmem((4, rows, 256), F32),
            vmem((8, rows, 128), BF16), vmem((8, rows, 128), BF16), vmem((6, rows, 128), BF16),
            vmem((4, rows // 2, 128), BF16), vmem((4, rows, 128), BF16), vmem((8, rows, 128), F32),
            dma((N_INPUTS,)), dma, dma((5,)), dma((5, HOPS)), dma((7,)), dma((7, HOPS)),
            dma((2,)), dma((2, 8)), dma((3,)), dma((3, 10)), dma((1,)), dma((7,)),
        ],
        compiler_params=pltpu.CompilerParams(
            collective_id=0, has_side_effects=True, vmem_limit_bytes=56 * 1024 * 1024),
        name="layer",
    )(*inputs)


def solution(mesh):
    return jax.shard_map(
        shards,
        mesh=mesh,
        in_specs=(
            P("fs", "tp"), P(), P("fs", "tp"), P("fs", "tp"), P("tp"), P("tp"), P("tp"),
            P("tp", None, None), P("tp", None), P("tp", "fs"), P("fs"), P(), P("fs", "tp"), P("tp"),
            P("tp", "fs"), P("fs"),
        ),
        out_specs=P("fs", "tp"),
        check_vma=False,
    )
```

time: 111 us -> 98.8 us (0.89)
  Pallas kernels: 106 us -> 96.7 us
  local copies, waits for them, and re-layouts: 4.96 us -> 1.62 us
    pallas_call x1, Pallas kernels: 106 us -> 96.7 us  [shards(): pl.pallas_call(layer_kernel, out_shape=jax.ShapeDtypeStruct((rows, width)...]
    unnamed x3 -> x1, local copies, waits for them, and re-layouts: 4.96 us -> 1.62 us
where the time goes in v2:
time: 98.8 us; the launch traced here: 98.3 us
  Pallas kernels  96.7 us (98%)
  local copies, waits for them, and re-layouts  1.62 us (2%)
    pallas_call x1, Pallas kernels, shards(): pl.pallas_call(layer_kernel, out_shape=jax.ShapeDtypeStruct((rows, width)...  96.7 us

profile of v2, /device:TPU:1, one launch (start us, length us, event | category | flops | bytes accessed | tf_op | source)
XLA Modules:
  0.0 98.3 jit_solution(9387689213504275208)
XLA Ops:
  0.0 96.7 %layer.1 = bf16[384,256]{1,0:T(8,128)(2,1)} custom-call(bf16[384,256]{1,0:T(8,128)(2,1)} %refs_0_.1, f32[1,2048]{1,0:T(1,128)} %bitcast.12, f32[32,128]{1,0:T(8,128)} %refs_2_.1, f32[32,128]{1,0:T(8,128)} %refs_3_.1, f32[1,128]{1,0:T(1,128)} %bitcast.15, f32[1,128]{1,0:T(1,128)} %bitcast.16, f32[1,128]{1,0:T(1,128)} %bitcast.17, ...), custom_call_target="tpu_custom_call" | custom-call | tf_op jit(solution)/shard_map/layer/pallas_call | solution.py:476
  96.7 1.6 %copy.18 = bf16[384,256]{1,0:T(8,128)(2,1)} copy(bf16[384,256]{1,0:T(8,128)(2,1)} %layer.1) | data formatting | bytes 393216

commit v3 on v2

--- a/solution.py
+++ b/solution.py
@@ -25,7 +25,7 @@
 
 def layer_kernel(*refs):
     hbm = refs[:N_INPUTS]
-    out_hbm = refs[N_INPUTS]
+    out_ref = refs[N_INPUTS]
     inputs = refs[N_INPUTS + 1:2 * N_INPUTS + 1]
     (
         tokens_ref, mixer_gain_ref, w_content_ref, w_spatial_ref, content_scale_ref, spatial_scale_ref,
@@ -33,10 +33,10 @@
         w_up_ref, up_scale_ref, w_down_ref, down_scale_ref,
     ) = inputs
     (
-        wa, wb, wu, wd0, wd1, tok1, tok2, normed, squares, hidden, partial, out_ref,
+        ws, wu, wd0, wd1, tok1, tok2, normed, squares, hidden,
         sib_out1, sib_in1, ring_out1, far_in1, near_in1, acc1,
         sib_out2, sib_in2, ring_out2, far_in2, near_in2, acc2,
-        in_sem, out_sem, w1_send, w1_recv, w2_send, w2_recv,
+        in_sem, w1_send, w1_recv, w2_send, w2_recv,
         ag_send, ag_recv, rs_send, rs_recv, sq_send, sq_recv,
     ) = refs[2 * N_INPUTS + 1:]
     fs, tp = lax.axis_index("fs"), lax.axis_index("tp")
@@ -53,10 +53,11 @@
         return 2 * ((x + dx + CHIPS_X) % CHIPS_X) + c
 
     first_next = (fs_of((p + 1) % RING, q), fs_of((p + RING - 1) % RING, q))
+    second_far = (fs_of(p, (q + 2) % RING), fs_of(p, (q + RING - 2) % RING))
     second_next = (fs_of(p, (q + 1) % RING), fs_of(p, (q + RING - 1) % RING))
 
     barrier = pltpu.get_barrier_semaphore()
-    for to in first_next + second_next:
+    for to in tuple(fs_of((p + d) % RING, q) for d in range(1, RING)) + second_next + second_far:
         pl.semaphore_signal(barrier, inc=1, device_id=(to, tp), device_id_type=MESH)
     for d in range(1, N_TP):
         pl.semaphore_signal(barrier, inc=1, device_id=(fs, (tp + d) % N_TP), device_id_type=MESH)
@@ -81,72 +82,99 @@
 
     for i in (2, 3, 9, 10):
         fetches[i].wait()
-    wa[q, p, :, 0:128] = w_content_ref[...].astype(BF16)
-    wa[q, p, :, 128:256] = w_spatial_ref[...].astype(BF16)
-    wb[q, p] = scaled(w_project_ref[...], project_scale_ref[...])
+    ws[q, 0, :, 0:128] = w_content_ref[...].astype(BF16)
+    ws[q, 0, :, 128:256] = w_spatial_ref[...].astype(BF16)
+    ws[q, 0, :, 256:384] = scaled(w_project_ref[...], project_scale_ref[...])
     for i in (0, 12, 14, 15):
         fetches[i].wait()
     tok1[tp] = tokens_ref[...]
     down = scaled(w_down_ref[...], down_scale_ref[...])
     for k in range(2):
         cols = slice(k * 512, (k + 1) * 512)
-        wu[k, q, p] = w_up_ref[:, cols].astype(BF16)
-        wd0[k, q, p] = down[0:16, cols]
-        wd1[k, q, p] = down[16:32, cols]
-    pl.semaphore_wait(barrier, 4 + N_TP - 1)
-
-    A, B, U, D0, D1 = range(5)
-    first_units = (wa, wb, wu, wd0, wd1)
-
-    def first_copy(u, way, step):
-        at = (p + (step if way else -step) + RING) % RING
-        if u in (A, B):
-            ref = first_units[u].at[q, at]
-            if step == HOPS - 1:
-                ref = ref.at[pl.ds(way * (SLICE // 2), SLICE // 2)]
-        elif step == HOPS - 1:
-            ref = first_units[u].at[way, q, at]
+        wu[k, q, 0] = w_up_ref[:, cols].astype(BF16)
+        wd0[k, q, 0] = down[0:16, cols]
+        wd1[k, q, 0] = down[16:32, cols]
+    pl.semaphore_wait(barrier, RING - 1 + 4 + N_TP - 1)
+
+    S, U, D0, D1 = range(4)
+    units = (ws, wu, wd0, wd1)
+
+    def first_copy(u, src, dst, to, sem, part=None):
+        if u == S:
+            src_ref, dst_ref = ws.at[q, src], ws.at[q, dst]
         else:
-            ref = first_units[u].at[:, q, at]
-        return remote(ref, ref, w1_send.at[u], w1_recv.at[u, step], first_next[way], tp)
+            lead = slice(None) if part is None else part
+            src_ref, dst_ref = units[u].at[lead, q, src], units[u].at[lead, q, dst]
+        return remote(src_ref, dst_ref, w1_send.at[u], w1_recv.at[u, sem], to, tp)
+
+    places = {0: 0, 1: 1, -1: 2, 2: 3, -2: 4, 3: 5, -3: 6, 4: 7, -4: 7}
 
     def first_send(u, step):
         for way in range(2):
-            first_copy(u, way, step).start()
-
-    def first_wait(u, step):
-        ref = first_units[u].at[0, 0] if u in (A, B) else first_units[u].at[:, 0, 0]
-        if step < HOPS - 1:
-            ref = first_units[u].at[0, 0:2] if u in (A, B) else first_units[u].at[:, 0, 0:2]
-        remote(ref, ref, w1_send.at[u], w1_recv.at[u, step], first_next[0], tp).wait_recv()
+            sign = 1 if way else -1
+            first_copy(u, places[sign * step], places[sign * (step + 1)], first_next[way], step,
+                       way if step == HOPS - 1 else None).start()
+
+    def small_send():
+        for d in (1, -1, 2, -2, 3, -3, 4):
+            first_copy(S, 0, places[-d], fs_of((p + d + RING) % RING, q), 0 if abs(d) == 1 else 1).start()
+
+    def small_wait(sem):
+        ref = ws.at[0, 0:2] if sem == 0 else ws.at[0, 0:5]
+        remote(ref, ref, w1_send.at[S], w1_recv.at[S, sem], first_next[0], tp).wait_recv()
+
+    def first_wait(u, distance):
+        n = 1 if distance == HOPS else 2
+        ref = units[u].at[:, 0, 0:n]
+        remote(ref, ref, w1_send.at[u], w1_recv.at[u, distance - 1], first_next[0], tp).wait_recv()
 
     def first_forward(u, step):
-        first_wait(u, step - 1)
+        first_wait(u, step)
         first_send(u, step)
 
-    U0, U1, E0, E1, E2 = 2, 3, 4, 5, 6
-    second_units = (wa, wb, wu.at[0], wu.at[1], wd0, wd1.at[0], wd1.at[1])
-
-    def second_copy(u, way, step):
+    Sa, Sb, Ua, Ub, D0a, D0b, D1a, D1b = range(8)
+
+    def group(g, at, lead=slice(None)):
+        shards_of = pl.ds(0, 3) if g % 2 == 0 else pl.ds(3, 5)
+        return ws.at[at, shards_of] if g < 2 else units[g // 2].at[lead, at, shards_of]
+
+    def second_copy(g, way, step):
         at = (q + (step if way else -step) + RING) % RING
-        ref = second_units[u].at[:, at] if u == E0 else second_units[u].at[at]
+        ref = group(g, at)
         if step == HOPS - 1:
-            rows = pl.ds(way * HOPS, HOPS)
-            ref = ref.at[:, rows] if u == E0 else ref.at[rows]
-        return remote(ref, ref, w2_send.at[u], w2_recv.at[u, step], second_next[way], tp)
-
-    def second_send(u, step=0):
+            ref = ref.at[:, pl.ds(way * (SLICE // 2), SLICE // 2)] if g < 2 else group(g, at, way)
+        return remote(ref, ref, w2_send.at[g], w2_recv.at[g, step], second_next[way], tp)
+
+    def far_copy(g, way, step):
+        at = (q + (2 * step if way else -2 * step) + RING) % RING
+        ref = group(g, at)
+        if step == 1:
+            ref = ref.at[:, pl.ds(way * (SLICE // 2), SLICE // 2)]
+        return remote(ref, ref, w2_send.at[g], w2_recv.at[g, 2 * step + 1], second_far[way], tp)
+
+    def two_stage(g, step):
+        if step == 1:
+            second_wait(g, 1)
         for way in range(2):
-            second_copy(u, way, step).start()
-
-    def second_wait(u, step=HOPS - 1):
-        n = 1 if step == HOPS - 1 else 2
-        ref = second_units[u].at[:, 0:n] if u == E0 else second_units[u].at[0:n]
-        remote(ref, ref, w2_send.at[u], w2_recv.at[u, step], second_next[0], tp).wait_recv()
-
-    def forward(u, step):
-        second_wait(u, step - 1)
-        second_send(u, step)
+            far_copy(g, way, step).start()
+        for way in range(2):
+            second_copy(g, way, 2 * step).start()
+
+    def two_stage_wait(g):
+        for step in (0, 2, 3):
+            second_wait(g, step)
+
+    def second_send(g, step=0):
+        for way in range(2):
+            second_copy(g, way, step).start()
+
+    def second_wait(g, step=HOPS - 1):
+        ref = group(g, 0) if step == HOPS - 1 else group(g, pl.ds(0, 2))
+        remote(ref, ref, w2_send.at[g], w2_recv.at[g, step], second_next[0], tp).wait_recv()
+
+    def forward(g, step):
+        second_wait(g, step - 1)
+        second_send(g, step)
 
     half = tokens_ref.shape[0] // 2
 
@@ -217,7 +245,6 @@
                 self.acc[k] = own
                 if k > 0:
                     self.own(k - 1)
-            self.own(3)
 
         def own(self, k):
             self.across(k).wait_recv()
@@ -243,6 +270,7 @@
                 self.near(way, way).start()
 
         def finish(self):
+            self.own(3)
             for way in range(2):
                 for part in range(2):
                     self.near(way, part).wait_recv()
@@ -266,7 +294,13 @@
             normed[:, cols] = (buf[t].astype(F32) * r * gain_ref[:, cols]).astype(BF16)
 
     def plane_rows(ref, zz, cols):
-        return [ref[jnp.where(core == 0, zz, j), jnp.where(core == 0, j, zz), :, cols] for j in range(RING)]
+        rows = []
+        for j in range(RING):
+            first, second = jnp.where(core == 0, j, zz), jnp.where(core == 0, zz, j)
+            d = (first - p + RING) % RING
+            at = jnp.where((d >= 1) & (d <= HOPS), 2 * d - 1, (2 * (RING - d)) % (2 * RING))
+            rows.append(ref[second, at, :, cols])
+        return rows
 
     def all_rows(ref, cols):
         return jnp.concatenate([r for zz in range(RING) for r in plane_rows(ref, zz, cols)], axis=0)
@@ -280,54 +314,46 @@
     scatter2 = Scatter(1, set_of(*bufs2, low=0), sib_out2.at[0:7])
     scatter3 = Scatter(2, set_of(*bufs2, low=1), sib_out2.at[0:7])
 
-    first_send(A, 0)
-    first_send(B, 0)
+    small_send()
     gather1.begin()
     first_send(U, 0)
     first_send(D0, 0)
     first_send(D1, 0)
-    first_forward(A, 1)
-    first_forward(B, 1)
+    small_wait(0)
+    two_stage(Sa, 0)
     first_forward(U, 1)
     first_forward(D0, 1)
     first_forward(D1, 1)
-    first_forward(A, 2)
-    first_forward(B, 2)
+    small_wait(1)
+    two_stage(Sb, 0)
+    gather1.pass_on()
     first_forward(U, 2)
+    second_send(Ua)
     first_forward(D0, 2)
     first_forward(D1, 2)
-    first_forward(A, 3)
-    first_forward(B, 3)
-    gather1.pass_on()
+    two_stage(Sa, 1)
+    second_send(D0a)
+    gather1.far()
     first_forward(U, 3)
     first_forward(D0, 3)
     first_forward(D1, 3)
-    first_wait(A, 3)
-    second_send(A)
-    first_wait(B, 3)
-    second_send(B)
+    two_stage(Sb, 1)
+    second_send(D1a)
+    forward(Ua, 1)
     for i in (1, 4, 5, 6, 7, 8, 11, 13):
         fetches[i].wait()
-    gather1.far()
-    first_wait(D1, 3)
-    second_send(E1)
     gather1.finish()
     normalize(tok1, mixer_gain_ref)
-    forward(A, 1)
-    forward(B, 1)
-    second_send(E2)
-    forward(A, 2)
-    forward(B, 2)
-    first_wait(U, 3)
-    first_wait(D0, 3)
-    forward(A, 3)
-    forward(B, 3)
-    second_send(U0)
-    second_send(U1)
-    second_send(E0)
-    second_wait(A)
-
-    linear = jnp.dot(normed[...], all_rows(wa, slice(0, 256)), preferred_element_type=F32)
+    first_wait(U, 4)
+    second_send(Ub)
+    first_wait(D0, 4)
+    second_send(D0b)
+    first_wait(D1, 4)
+    second_send(D1b)
+    two_stage_wait(Sa)
+    two_stage_wait(Sb)
+
+    linear = jnp.dot(normed[...], all_rows(ws, slice(0, 256)), preferred_element_type=F32)
     spatial = jax.nn.gelu(linear[:, 128:256] * spatial_scale_ref[...])
     sq = spatial * spatial
     sq_high = sq.astype(BF16)
@@ -349,6 +375,8 @@
     )
     mixing = jnp.where(causal, mixing_ref[0].astype(F32), 0.0)
     bias = jnp.transpose(jnp.broadcast_to(bias_ref[...], (BLOCK, BLOCK)))
+    forward(D0a, 1)
+    forward(D1a, 1)
     for d in range(1, N_TP):
         square_copy(d, True).wait_recv()
     total_sq = squares[0]
@@ -365,30 +393,33 @@
 
     def project_blocks(k, dx):
         return tuple(
-            nt_dot(gated, jnp.concatenate(plane_rows(wb, tp_of(dx, other), slice(0, 128)), axis=0))
+            nt_dot(gated, jnp.concatenate(plane_rows(ws, tp_of(dx, other), slice(256, 384)), axis=0))
             for other in (True, False))
 
-    forward(U0, 1)
-    second_wait(B)
+    forward(Ub, 1)
     scatter1.begin(project_blocks)
-    forward(U1, 1)
+    forward(D0b, 1)
+    forward(Ua, 2)
+    forward(D1b, 1)
     scatter1.combine()
-    forward(E0, 1)
-    forward(U0, 2)
+    forward(D0a, 2)
+    forward(Ub, 2)
     middle = (tokens_ref[...].astype(F32) + scatter1.finish()).astype(BF16)
     tok2[tp] = middle
     gather2.begin()
-    forward(U1, 2)
-    forward(E0, 2)
+    forward(D0b, 2)
+    forward(Ua, 3)
+    forward(D1a, 2)
+    forward(D1b, 2)
+    forward(D0a, 3)
     gather2.pass_on()
-    forward(U0, 3)
-    forward(E1, 1)
+    forward(Ub, 3)
     gather2.far()
-    forward(E2, 1)
+    forward(D0b, 3)
     gather2.finish()
-    forward(U1, 3)
+    forward(D1a, 3)
+    forward(D1b, 3)
     normalize(tok2, channel_gain_ref)
-    forward(E0, 3)
 
     def up_tiles(k):
         for low in range(0, 512, 256):
@@ -397,12 +428,10 @@
             up = jnp.maximum(up * up_scale_ref[:, at:at + 256], 0.0)
             hidden[:, at:at + 256] = (up * up).astype(BF16)
 
-    second_wait(U0)
+    second_wait(Ua)
+    second_wait(Ub)
     up_tiles(0)
-    forward(E1, 2)
-    second_wait(U1)
     up_tiles(1)
-    forward(E2, 2)
 
     natural = lax.broadcasted_iota(jnp.int32, (width, width), 0)
     split = lax.broadcasted_iota(jnp.int32, (width, width), 1)
@@ -415,48 +444,38 @@
         pieces = [r for other in (True, False) for r in plane_rows(ref.at[k], tp_of(dx, other), slice(0, 512))]
         return nt_dot(hidden[:, k * 512:(k + 1) * 512], jnp.concatenate(pieces, axis=0))
 
-    def first_half(k, dx):
-        both = down_pair(wd0, 0, dx) + down_pair(wd0, 1, dx)
-        return both[:, 0:128], both[:, 128:256]
-
-    def second_half(k, dx):
-        both = partial[k] + down_pair(wd1, 1, dx)
-        return both[:, 0:128], both[:, 128:256]
-
-    second_wait(E0)
-    scatter2.begin(first_half)
-    forward(E1, 3)
-    forward(E2, 3)
+    def down_half(ref):
+        def blocks(k, dx):
+            both = down_pair(ref, 0, dx) + down_pair(ref, 1, dx)
+            return both[:, 0:128], both[:, 128:256]
+
+        return blocks
+
+    second_wait(D0a)
+    second_wait(D0b)
+    scatter2.begin(down_half(wd0))
+    second_wait(D1a)
+    second_wait(D1b)
+    scatter3.begin(down_half(wd1))
     scatter2.combine()
-    second_wait(E1)
-    for k, dx in enumerate(Scatter.order):
-        partial[k] = down_pair(wd1, 0, dx)
-    second_wait(E2)
-    scatter3.begin(second_half)
+    scatter3.combine()
     half0 = (middle_split[:, 0:128] + scatter2.finish()).astype(BF16)
     out0 = nt_dot(half0, order[:, 0:128])
-    scatter3.combine()
     half1 = (middle_split[:, 128:256] + scatter3.finish()).astype(BF16)
     out_ref[...] = (out0 + nt_dot(half1, order[:, 128:256])).astype(BF16)
-    store = pltpu.make_async_copy(out_ref, out_hbm, out_sem)
-    store.start()
-
-    for u in (A, B):
-        ref = first_units[u].at[0, 0:7]
+
+    for u in range(4):
+        ref = ws.at[0, 0:7] if u == S else units[u].at[:, 0, 0:7]
         remote(ref, ref, w1_send.at[u], w1_recv.at[u, 0], fs, tp_of(1, False)).wait_send()
-    for u in (U, D0, D1):
-        ref = first_units[u].at[:, 0, 0:7]
-        remote(ref, ref, w1_send.at[u], w1_recv.at[u, 0], fs, tp_of(1, False)).wait_send()
-    for u in range(7):
-        ref = second_units[u].at[:, 0:7] if u == E0 else second_units[u].at[0:7]
-        remote(ref, ref, w2_send.at[u], w2_recv.at[u, 0], fs, tp_of(1, False)).wait_send()
+    for g in range(8):
+        ref = group(g, pl.ds(0, 7))
+        remote(ref, ref, w2_send.at[g], w2_recv.at[g, 0], fs, tp_of(1, False)).wait_send()
     gather1.drain()
     gather2.drain()
     scatter1.drain()
     scatter2.drain()
     scatter3.drain()
     remote(squares.at[0:7], squares.at[0:7], sq_send.at[0], sq_recv.at[0], fs, tp_of(1, False)).wait_send()
-    store.wait()
 
 
 def shards(
@@ -475,12 +494,11 @@
     anywhere = pl.BlockSpec(memory_space=pl.ANY)
     return pl.pallas_call(
         layer_kernel,
-        out_shape=jax.ShapeDtypeStruct((rows, width), BF16),
+        out_shape=pltpu.VMEM((rows, width), BF16),
         in_specs=[anywhere] * N_INPUTS,
-        out_specs=anywhere,
+        out_specs=pl.BlockSpec(memory_space=pltpu.VMEM),
         scratch_shapes=[vmem(v.shape, v.dtype) for v in inputs] + [
-            vmem((RING, RING, SLICE, 256), BF16),
-            vmem((RING, RING, SLICE, 128), BF16),
+            vmem((RING, RING, SLICE, 384), BF16),
             vmem((2, RING, RING, SLICE, 512), BF16),
             vmem((2, RING, RING, SLICE // 2, 512), BF16),
             vmem((2, RING, RING, SLICE // 2, 512), BF16),
@@ -489,13 +507,11 @@
             vmem((rows, N_TP * width), BF16),
             vmem((N_TP, 8, rows), F32),
             vmem((rows, w_up.shape[1]), BF16),
-            vmem((4, rows, width), F32),
-            vmem((rows, width), BF16),
             vmem((4, rows, 256), BF16), vmem((4, rows, 256), BF16), vmem((3, rows, 256), BF16),
             vmem((2, rows // 2, 256), BF16), vmem((2, rows, 256), BF16), vmem((4, rows, 256), F32),
             vmem((8, rows, 128), BF16), vmem((8, rows, 128), BF16), vmem((6, rows, 128), BF16),
             vmem((4, rows // 2, 128), BF16), vmem((4, rows, 128), BF16), vmem((8, rows, 128), F32),
-            dma((N_INPUTS,)), dma, dma((5,)), dma((5, HOPS)), dma((7,)), dma((7, HOPS)),
+            dma((N_INPUTS,)), dma((4,)), dma((4, HOPS)), dma((8,)), dma((8, HOPS)),
             dma((2,)), dma((2, 8)), dma((3,)), dma((3, 10)), dma((1,)), dma((7,)),
         ],
         compiler_params=pltpu.CompilerParams(

time: 98.8 us -> 89.9 us (0.910)
  Pallas kernels: 96.7 us -> 89 us
    pallas_call x1, Pallas kernels: 96.7 us -> 89 us  [shards(): pl.pallas_call(layer_kernel, out_shape=pltpu.VMEM((rows, width), BF16), i...]
where the time goes in v3:
time: 89.9 us; the launch traced here: 89.7 us
  Pallas kernels  89 us (99%)
    pallas_call x1, Pallas kernels, shards(): pl.pallas_call(layer_kernel, out_shape=pltpu.VMEM((rows, width), BF16), i...  89 us

profile of v3, /device:TPU:1, one launch (start us, length us, event | category | flops | bytes accessed | tf_op | source)
XLA Modules:
  0.0 89.7 jit_solution(16065357459530395415)
XLA Ops:
  0.0 89.0 %layer.1 = bf16[384,256]{1,0:T(8,128)(2,1)S(1)} custom-call(bf16[384,256]{1,0:T(8,128)(2,1)} %refs_0_.1, f32[1,2048]{1,0:T(1,128)} %bitcast.12, f32[32,128]{1,0:T(8,128)} %refs_2_.1, f32[32,128]{1,0:T(8,128)} %refs_3_.1, f32[1,128]{1,0:T(1,128)} %bitcast.15, f32[1,128]{1,0:T(1,128)} %bitcast.16, f32[1,128]{1,0:T(1,128)} %bitcast.17, ...), custom_call_target="tpu_custom_call" | custom-call | tf_op jit(solution)/shard_map/layer/pallas_call | solution.py:495
  89.0 0.7 copy.18

commit v4 on v3

v4 whole, which is shorter than its diff:
```python
import jax
import jax.numpy as jnp
from jax import lax
from jax.experimental import pallas as pl
from jax.experimental.pallas import tpu as pltpu
from jax.sharding import PartitionSpec as P

EPSILON = 1e-06
MESH = pl.DeviceIdType.MESH
F32 = jnp.float32
BF16 = jnp.bfloat16

RING = 8
HOPS = RING // 2
CHIPS_X = 4
N_TP = 2 * CHIPS_X
SLICE = 32
BLOCK = 128
N_INPUTS = 16


def nt_dot(left, right):
    return lax.dot_general(left, right, (((1,), (1,)), ((), ())), preferred_element_type=F32)


def layer_kernel(*refs):
    hbm = refs[:N_INPUTS]
    out_ref = refs[N_INPUTS]
    inputs = refs[N_INPUTS + 1:2 * N_INPUTS + 1]
    (
        tokens_ref, mixer_gain_ref, w_content_ref, w_spatial_ref, content_scale_ref, spatial_scale_ref,
        spatial_gain_ref, mixing_ref, bias_ref, w_project_ref, project_scale_ref, channel_gain_ref,
        w_up_ref, up_scale_ref, w_down_ref, down_scale_ref,
    ) = inputs
    (
        wp, wc, wu, wd0, wd1, tok1, tok2, normed, squares, hidden, up_acc,
        sib_out1, sib_in1, ring_out1, far_in1, near_in1, acc1,
        sib_out2, sib_in2, ring_out2, far_in2, near_in2, acc2,
        in_sem, w1_send, w1_recv, w2_send, w2_recv,
        ag_send, ag_recv, rs_send, rs_recv, sq_send, sq_recv,
    ) = refs[2 * N_INPUTS + 1:]
    fs, tp = lax.axis_index("fs"), lax.axis_index("tp")
    z, y = fs // RING, fs % RING
    x, core = tp // 2, tp % 2
    p = jnp.where(core == 0, y, z)
    q = jnp.where(core == 0, z, y)

    def fs_of(pp, qq):
        return jnp.where(core == 0, qq * RING + pp, pp * RING + qq)

    def tp_of(dx, other):
        c = (1 - core) if other else core
        return 2 * ((x + dx + CHIPS_X) % CHIPS_X) + c

    first_next = (fs_of((p + 1) % RING, q), fs_of((p + RING - 1) % RING, q))
    second_next = (fs_of(p, (q + 1) % RING), fs_of(p, (q + RING - 1) % RING))

    barrier = pltpu.get_barrier_semaphore()
    for to in tuple(fs_of((p + d) % RING, q) for d in range(1, RING)) + second_next:
        pl.semaphore_signal(barrier, inc=1, device_id=(to, tp), device_id_type=MESH)
    for d in range(1, N_TP):
        pl.semaphore_signal(barrier, inc=1, device_id=(fs, (tp + d) % N_TP), device_id_type=MESH)
    fetches = [pltpu.make_async_copy(hbm[i], inputs[i], in_sem.at[i]) for i in range(N_INPUTS)]
    for i in (2, 3, 9, 10, 0, 12, 14, 15, 1, 4, 5, 6, 7, 8, 11, 13):
        fetches[i].start()

    def remote(src, dst, ss, rs, to_fs, to_tp):
        return pltpu.make_async_remote_copy(
            src_ref=src, dst_ref=dst, send_sem=ss, recv_sem=rs,
            device_id=(to_fs, to_tp), device_id_type=MESH,
        )

    eye = (
        lax.broadcasted_iota(jnp.int32, (SLICE, SLICE), 0)
        == lax.broadcasted_iota(jnp.int32, (SLICE, SLICE), 1)
    )

    def scaled(w, scale):
        column = jnp.sum(jnp.where(eye, scale, 0.0), axis=1, keepdims=True)
        return (w.astype(BF16).astype(F32) * column).astype(BF16)

    for i in (2, 3, 9, 10):
        fetches[i].wait()
    wp[q, 0] = w_spatial_ref[...].astype(BF16)
    wc[q, 0, :, 0:128] = w_content_ref[...].astype(BF16)
    wc[q, 0, :, 128:256] = scaled(w_project_ref[...], project_scale_ref[...])
    for i in (0, 12, 14, 15):
        fetches[i].wait()
    tok1[tp] = tokens_ref[...]
    down = scaled(w_down_ref[...], down_scale_ref[...])
    for k in range(2):
        cols = slice(k * 512, (k + 1) * 512)
        wu[k, q, 0] = w_up_ref[:, cols].astype(BF16)
        wd0[k, q, 0] = down[0:16, cols]
        wd1[k, q, 0] = down[16:32, cols]
    pl.semaphore_wait(barrier, RING - 1 + 2 + N_TP - 1)

    SP, SC, U, D0, D1 = range(5)
    units = (wp, wc, wu, wd0, wd1)

    def first_copy(u, src, dst, to, sem, part=None):
        if u <= SC:
            src_ref, dst_ref = units[u].at[q, src], units[u].at[q, dst]
        else:
            lead = slice(None) if part is None else part
            src_ref, dst_ref = units[u].at[lead, q, src], units[u].at[lead, q, dst]
        return remote(src_ref, dst_ref, w1_send.at[u], w1_recv.at[u, sem], to, tp)

    places = {0: 0, 1: 1, -1: 2, 2: 3, -2: 4, 3: 5, -3: 6, 4: 7, -4: 7}

    def first_send(u, step):
        for way in range(2):
            sign = 1 if way else -1
            first_copy(u, places[sign * step], places[sign * (step + 1)], first_next[way], step,
                       way if step == HOPS - 1 else None).start()

    def small_send(u):
        for d in (1, -1, 2, -2, 3, -3, 4):
            first_copy(u, 0, places[-d], fs_of((p + d + RING) % RING, q), 0 if abs(d) == 1 else 1).start()

    def small_wait(u, sem):
        ref = units[u].at[0, 0:2] if sem == 0 else units[u].at[0, 0:5]
        remote(ref, ref, w1_send.at[u], w1_recv.at[u, sem], first_next[0], tp).wait_recv()

    def first_wait(u, distance=HOPS):
        n = 1 if distance == HOPS else 2
        ref = units[u].at[:, 0, 0:n]
        remote(ref, ref, w1_send.at[u], w1_recv.at[u, distance - 1], first_next[0], tp).wait_recv()

    def first_forward(u, step):
        first_wait(u, step)
        first_send(u, step)

    SPa, SPb, SCa, SCb, Ua, Ub, D0a, D0b, D1a, D1b = range(10)
    SMALL = 4

    def group(g, at, lead=slice(None)):
        shards_of = pl.ds(0, 3) if g % 2 == 0 else pl.ds(3, 5)
        return units[g // 2].at[at, shards_of] if g < SMALL else units[g // 2].at[lead, at, shards_of]

    def second_copy(g, way, step):
        at = (q + (step if way else -step) + RING) % RING
        ref = group(g, at)
        if step == HOPS - 1:
            ref = ref.at[:, pl.ds(way * (SLICE // 2), SLICE // 2)] if g < SMALL else group(g, at, way)
        return remote(ref, ref, w2_send.at[g], w2_recv.at[g, step], second_next[way], tp)

    def second_send(g, step=0):
        for way in range(2):
            second_copy(g, way, step).start()

    def second_wait(g, step=HOPS - 1):
        ref = group(g, 0) if step == HOPS - 1 else group(g, pl.ds(0, 2))
        remote(ref, ref, w2_send.at[g], w2_recv.at[g, step], second_next[0], tp).wait_recv()

    def forward(g, step):
        second_wait(g, step - 1)
        second_send(g, step)

    half = tokens_ref.shape[0] // 2

    class Gather:
        def __init__(self, buf, n):
            self.buf, self.n = buf, n

        def copy(self, k, arriving=False):
            dx = (0, -1, 1, 2, 0, 0, 0, 0, -1, 1)[k]
            if arriving and k >= 4:
                dx = (-1, 1, -1, 1, -2, 2)[k - 4]
            ref = self.buf.at[tp_of(dx, arriving and k < 4)]
            if k >= 4:
                ref = ref.at[pl.ds((k % 2 if k // 2 != 3 else 1 - k % 2) * half, half)]
            to = tp_of(0, True) if k < 4 else tp_of((1, -1)[k % 2], False)
            return remote(ref, ref, ag_send.at[self.n], ag_recv.at[self.n, k], fs, to)

        def begin(self):
            for k in (4, 5, 6, 7, 0):
                self.copy(k).start()

        def pass_on(self):
            for k in range(2):
                self.copy(4 + k, True).wait_recv()
                self.copy(8 + k).start()

        def near(self):
            for k in range(2):
                self.copy(6 + k, True).wait_recv()
                self.copy(1 + k).start()

        def far(self):
            for k in range(2):
                self.copy(8 + k, True).wait_recv()
            self.copy(3).start()

        def wait(self, *which):
            for k in which:
                self.copy(k, True).wait_recv()

        def drain(self):
            ref = self.buf.at[0:7]
            remote(ref, ref, ag_send.at[self.n], ag_recv.at[self.n, 0], fs, tp_of(1, False)).wait_send()

    class Scatter:
        order = (2, 1, -1, 0)

        def __init__(self, n, bufs, bytes_ref):
            self.n, self.bytes_ref = n, bytes_ref
            self.sib_out, self.sib_in, self.ring_out, self.far_in, self.near_in, self.acc = bufs

        def copy(self, src, dst, k, to):
            return remote(src, dst, rs_send.at[self.n], rs_recv.at[self.n, k], fs, to)

        def across(self, k):
            return self.copy(self.sib_out.at[k], self.sib_in.at[k], k, tp_of(0, True))

        def far(self, way):
            return self.copy(self.ring_out.at[0, pl.ds(way * half, half)], self.far_in.at[way], 4 + way,
                             tp_of((1, -1)[way], False))

        def near(self, way, part):
            rows = pl.ds(part * half, half)
            return self.copy(self.ring_out.at[1 + way, rows], self.near_in.at[way, rows], 6 + 2 * way + part,
                             tp_of((1, -1)[way], False))

        def begin(self, blocks_of):
            for k, dx in enumerate(self.order):
                across, own = blocks_of(k, dx)
                self.sib_out[k] = across.astype(BF16)
                self.across(k).start()
                self.acc[k] = own
                if k > 0:
                    self.own(k - 1)

        def own(self, k):
            self.across(k).wait_recv()
            value = self.acc[k] + self.sib_in[k].astype(F32)
            if k == 0:
                self.ring_out[0] = value.astype(BF16)
                self.far(0).start()
                self.far(1).start()
            else:
                self.acc[k] = value
                if k < 3:
                    part = 2 - k
                    rows = slice(part * half, (part + 1) * half)
                    self.ring_out[k, rows] = value[rows].astype(BF16)
                    self.near(k - 1, part).start()

        def combine(self):
            for way in range(2):
                self.far(way).wait_recv()
                rows = slice(way * half, (way + 1) * half)
                self.ring_out[1 + way, rows] = (
                    self.acc[1 + way, rows] + self.far_in[way].astype(F32)).astype(BF16)
                self.near(way, way).start()

        def finish(self):
            self.own(3)
            for way in range(2):
                for part in range(2):
                    self.near(way, part).wait_recv()
            return self.acc[3] + self.near_in[0].astype(F32) + self.near_in[1].astype(F32)

        def drain(self):
            remote(self.bytes_ref, self.bytes_ref, rs_send.at[self.n], rs_recv.at[self.n, 0], fs,
                   tp_of(1, False)).wait_send()

    width = tokens_ref.shape[1]

    def normalize():
        total = None
        for t in range(N_TP):
            v = tok1[t].astype(F32)
            s = jnp.sum(v * v, axis=1, keepdims=True)
            total = s if total is None else total + s
        r = lax.rsqrt(total / (N_TP * width) + EPSILON)
        for t in range(N_TP):
            cols = slice(t * width, (t + 1) * width)
            normed[:, cols] = (tok1[t].astype(F32) * r * mixer_gain_ref[:, cols]).astype(BF16)

    def plane_rows(ref, zz, cols):
        rows = []
        for j in range(RING):
            first, second = jnp.where(core == 0, j, zz), jnp.where(core == 0, zz, j)
            d = (first - p + RING) % RING
            at = jnp.where((d >= 1) & (d <= HOPS), 2 * d - 1, (2 * (RING - d)) % (2 * RING))
            rows.append(ref[second, at, :, cols])
        return rows

    def all_rows(ref, cols):
        return jnp.concatenate([r for zz in range(RING) for r in plane_rows(ref, zz, cols)], axis=0)

    def set_of(*bufs, low=None):
        return bufs if low is None else tuple(b.at[pl.ds(low * (b.shape[0] // 2), b.shape[0] // 2)] for b in bufs)

    gather1, gather2 = Gather(tok1, 0), Gather(tok2, 1)
    bufs2 = (sib_out2, sib_in2, ring_out2, far_in2, near_in2, acc2)
    scatter1 = Scatter(0, (sib_out1, sib_in1, ring_out1, far_in1, near_in1, acc1), tok1.at[0:7])
    scatter2 = Scatter(1, set_of(*bufs2, low=0), sib_out2.at[0:7])
    scatter3 = Scatter(2, set_of(*bufs2, low=1), sib_out2.at[0:7])

    value = {}

    def square_copy(d, arriving=False):
        ref = squares.at[(tp + N_TP - d) % N_TP] if arriving else squares.at[tp]
        return remote(ref, ref, sq_send.at[0], sq_recv.at[d - 1], fs, (tp + d) % N_TP)

    def spatial_branch():
        linear = jnp.dot(normed[...], all_rows(wp, slice(0, 128)), preferred_element_type=F32)
        spatial = jax.nn.gelu(linear * spatial_scale_ref[...])
        sq = spatial * spatial
        sq_high = sq.astype(BF16)
        sq_low = (sq - sq_high.astype(F32)).astype(BF16)
        ones = jnp.ones((8, 128), BF16)
        squares[tp] = nt_dot(ones, sq_high) + nt_dot(ones, sq_low)
        for d in range(1, N_TP):
            square_copy(d).start()
        value["gained"] = (spatial * spatial_gain_ref[...]).astype(BF16)

    def content_branch():
        linear = jnp.dot(normed[...], all_rows(wc, slice(0, 128)), preferred_element_type=F32)
        value["content"] = jax.nn.gelu(linear * content_scale_ref[...])
        causal = (
            lax.broadcasted_iota(jnp.int32, (BLOCK, BLOCK), 1)
            <= lax.broadcasted_iota(jnp.int32, (BLOCK, BLOCK), 0)
        )
        value["mixing"] = jnp.where(causal, mixing_ref[0].astype(F32), 0.0)
        value["bias"] = jnp.transpose(jnp.broadcast_to(bias_ref[...], (BLOCK, BLOCK)))

    def square_wait():
        for d in range(1, N_TP):
            square_copy(d, True).wait_recv()

    def mix():
        total_sq = squares[0]
        for t in range(1, N_TP):
            total_sq = total_sq + squares[t]
        row_scale = lax.rsqrt(total_sq[0:1] / (N_TP * 128) + EPSILON)
        gated = []
        for b in range(tokens_ref.shape[0] // BLOCK):
            rows = slice(b * BLOCK, (b + 1) * BLOCK)
            mixing_b = (value["mixing"] * row_scale[:, rows]).astype(BF16)
            mixed = jnp.dot(mixing_b, value["gained"][rows], preferred_element_type=F32) + value["bias"]
            gated.append((value["content"][rows] * mixed).astype(BF16))
        value["gated"] = jnp.concatenate(gated, axis=0)

    def project_blocks(k, dx):
        return tuple(
            nt_dot(value["gated"], jnp.concatenate(plane_rows(wc, tp_of(dx, other), slice(128, 256)), axis=0))
            for other in (True, False))

    def middle():
        value["middle"] = (tokens_ref[...].astype(F32) + scatter1.finish()).astype(BF16)
        tok2[tp] = value["middle"]
        gather2.begin()

    def up_part(dxs, first=False):
        blocks = [tp_of(dx, other) for dx in dxs for other in (False, True)]
        terms = []
        for t in blocks:
            v = tok2[t].astype(F32)
            s = jnp.sum(v * v, axis=1, keepdims=True)
            value["sum"] = s if first and not terms else value["sum"] + s
            gain = channel_gain_ref[:, pl.ds(pl.multiple_of(t * width, 128), width)]
            terms.append((v * gain).astype(BF16))
        left = jnp.concatenate(terms, axis=1)
        for k in range(2):
            for low in range(0, 512, 256):
                cols = slice(low, low + 256)
                right = jnp.concatenate([r for t in blocks for r in plane_rows(wu.at[k], t, cols)], axis=0)
                at = slice(k * 512 + low, k * 512 + low + 256)
                part = jnp.dot(left, right, preferred_element_type=F32)
                up_acc[:, at] = part if first else up_acc[:, at] + part

    def activate():
        r = lax.rsqrt(value["sum"] / (N_TP * width) + EPSILON)
        up = jnp.maximum(up_acc[...] * r * up_scale_ref[...], 0.0)
        hidden[...] = (up * up).astype(BF16)

    def split_middle():
        natural = lax.broadcasted_iota(jnp.int32, (width, width), 0)
        split = lax.broadcasted_iota(jnp.int32, (width, width), 1)
        value["order"] = (
            natural == ((split % 128) // 16) * 32 + (split // 128) * 16 + split % 16
        ).astype(F32).astype(BF16)
        value["split"] = jnp.dot(value["middle"], value["order"], preferred_element_type=F32)

    def down_half(ref):
        def pair(k, blocks):
            pieces = [r for zz in blocks for r in plane_rows(ref.at[k], zz, slice(0, 512))]
            return nt_dot(hidden[:, k * 512:(k + 1) * 512], jnp.concatenate(pieces, axis=0))

        def blocks_of(k, dx):
            blocks = [tp_of(dx, other) for other in (True, False)]
            both = pair(0, blocks) + pair(1, blocks)
            return both[:, 0:128], both[:, 128:256]

        return blocks_of

    def half_out(scatter, cols):
        rounded = (value["split"][:, cols] + scatter.finish()).astype(BF16)
        return nt_dot(rounded, value["order"][:, cols])

    def first_out():
        value["out"] = half_out(scatter2, slice(0, 128))

    def second_out():
        out_ref[...] = (value["out"] + half_out(scatter3, slice(128, 256))).astype(BF16)

    def late_fetches():
        for i in (1, 4, 5, 6, 7, 8, 11, 13):
            fetches[i].wait()

    first_send(D0, 0)
    first_send(D1, 0)
    small_send(SP)
    small_send(SC)
    gather1.begin()
    first_send(U, 0)
    first_forward(D1, 1)
    second_send(D1a)
    first_forward(D0, 1)
    second_send(D0a)
    small_wait(SC, 0)
    small_wait(SP, 0)
    second_send(SPa)
    small_wait(SP, 1)
    gather1.pass_on()
    second_send(SCa)
    second_send(SPb)
    first_forward(U, 1)
    small_wait(SC, 1)
    gather1.near()
    second_send(SCb)
    second_send(Ua)
    first_forward(D1, 2)
    gather1.far()
    forward(SPa, 1)
    first_forward(U, 2)
    forward(SPb, 1)
    gather1.wait(0, 1, 2, 3)
    forward(SCa, 1)
    forward(SCb, 1)
    forward(D0a, 1)
    first_forward(D0, 2)
    late_fetches()
    normalize()
    forward(SPa, 2)
    forward(SPb, 2)
    forward(Ua, 1)
    first_forward(U, 3)
    first_forward(D1, 3)
    first_forward(D0, 3)
    forward(D1a, 1)
    forward(SCa, 2)
    forward(SCb, 2)
    first_wait(U)
    forward(SPa, 3)
    forward(SPb, 3)
    second_send(Ub)
    first_wait(D1)
    forward(SCa, 3)
    forward(SCb, 3)
    second_wait(SPa)
    second_wait(SPb)
    forward(Ua, 2)
    forward(D1a, 2)
    spatial_branch()
    second_send(D1b)
    first_wait(D0)
    second_wait(SCa)
    second_wait(SCb)
    content_branch()
    forward(Ub, 1)
    square_wait()
    second_send(D0b)
    mix()
    forward(D0a, 2)
    scatter1.begin(project_blocks)
    forward(D1b, 1)
    forward(Ub, 2)
    scatter1.combine()
    forward(D0b, 1)
    middle()
    forward(Ua, 3)
    forward(D1b, 2)
    forward(Ub, 3)
    split_middle()
    gather2.wait(0)
    gather2.pass_on()
    gather2.near()
    forward(D0b, 2)
    forward(D1b, 3)
    forward(D1a, 3)
    gather2.wait(1, 2)
    gather2.far()
    second_wait(Ua)
    second_wait(Ub)
    forward(D0a, 3)
    up_part((0,), True)
    up_part((-1, 1))
    gather2.wait(3)
    forward(D0b, 3)
    up_part((2,))
    second_wait(D1b)
    activate()
    second_wait(D1a)
    scatter3.begin(down_half(wd1))
    second_wait(D0b)
    second_wait(D0a)
    scatter2.begin(down_half(wd0))
    scatter3.combine()
    scatter2.combine()
    first_out()
    second_out()
    for u in range(5):
        ref = units[u].at[0, 0:7] if u <= SC else units[u].at[:, 0, 0:7]
        remote(ref, ref, w1_send.at[u], w1_recv.at[u, 0], fs, tp_of(1, False)).wait_send()
    for g in range(10):
        ref = group(g, pl.ds(0, 7))
        remote(ref, ref, w2_send.at[g], w2_recv.at[g, 0], fs, tp_of(1, False)).wait_send()
    gather1.drain()
    gather2.drain()
    scatter1.drain()
    scatter2.drain()
    scatter3.drain()
    remote(squares.at[0:7], squares.at[0:7], sq_send.at[0], sq_recv.at[0], fs, tp_of(1, False)).wait_send()


def shards(
    tokens, mixer_gain, w_content, w_spatial, content_scale, spatial_scale, spatial_gain, block_mixing,
    block_bias, w_project, project_scale, channel_gain, w_up, up_scale, w_down, down_scale,
):
    rows, width = tokens.shape
    row = lambda v: v.reshape(1, -1)
    inputs = (
        tokens, row(mixer_gain), w_content, w_spatial, row(content_scale), row(spatial_scale),
        row(spatial_gain), block_mixing, block_bias, w_project.T, row(project_scale), row(channel_gain),
        w_up, row(up_scale), w_down.T, row(down_scale),
    )
    vmem = pltpu.VMEM
    dma = pltpu.SemaphoreType.DMA
    anywhere = pl.BlockSpec(memory_space=pl.ANY)
    return pl.pallas_call(
        layer_kernel,
        out_shape=pltpu.VMEM((rows, width), BF16),
        in_specs=[anywhere] * N_INPUTS,
        out_specs=pl.BlockSpec(memory_space=pltpu.VMEM),
        scratch_shapes=[vmem(v.shape, v.dtype) for v in inputs] + [
            vmem((RING, RING, SLICE, 128), BF16),
            vmem((RING, RING, SLICE, 256), BF16),
            vmem((2, RING, RING, SLICE, 512), BF16),
            vmem((2, RING, RING, SLICE // 2, 512), BF16),
            vmem((2, RING, RING, SLICE // 2, 512), BF16),
            vmem((N_TP, rows, width), BF16),
            vmem((N_TP, rows, width), BF16),
            vmem((rows, N_TP * width), BF16),
            vmem((N_TP, 8, rows), F32),
            vmem((rows, w_up.shape[1]), BF16),
            vmem((rows, w_up.shape[1]), F32),
            vmem((4, rows, 256), BF16), vmem((4, rows, 256), BF16), vmem((3, rows, 256), BF16),
            vmem((2, rows // 2, 256), BF16), vmem((2, rows, 256), BF16), vmem((4, rows, 256), F32),
            vmem((8, rows, 128), BF16), vmem((8, rows, 128), BF16), vmem((6, rows, 128), BF16),
            vmem((4, rows // 2, 128), BF16), vmem((4, rows, 128), BF16), vmem((8, rows, 128), F32),
            dma((N_INPUTS,)), dma((5,)), dma((5, HOPS)), dma((10,)), dma((10, HOPS)),
            dma((2,)), dma((2, 10)), dma((3,)), dma((3, 10)), dma((1,)), dma((7,)),
        ],
        compiler_params=pltpu.CompilerParams(
            collective_id=0, has_side_effects=True, vmem_limit_bytes=56 * 1024 * 1024),
        name="layer",
    )(*inputs)


def solution(mesh):
    return jax.shard_map(
        shards,
        mesh=mesh,
        in_specs=(
            P("fs", "tp"), P(), P("fs", "tp"), P("fs", "tp"), P("tp"), P("tp"), P("tp"),
            P("tp", None, None), P("tp", None), P("tp", "fs"), P("fs"), P(), P("fs", "tp"), P("tp"),
            P("tp", "fs"), P("fs"),
        ),
        out_specs=P("fs", "tp"),
        check_vma=False,
    )
```

time: 89.9 us -> 86.5 us (0.962)
  Pallas kernels: 89 us -> 85.6 us
    pallas_call x1, Pallas kernels: 89 us -> 85.6 us  [shards(): pl.pallas_call(layer_kernel, out_shape=pltpu.VMEM((rows, width), BF16), i...]
where the time goes in v4:
time: 86.5 us; the launch traced here: 86.3 us
  Pallas kernels  85.6 us (99%)
    pallas_call x1, Pallas kernels, shards(): pl.pallas_call(layer_kernel, out_shape=pltpu.VMEM((rows, width), BF16), i...  85.6 us

profile of v4, /device:TPU:1, one launch (start us, length us, event | category | flops | bytes accessed | tf_op | source)
XLA Modules:
  0.0 86.3 jit_solution(5703293584097013452)
XLA Ops:
  0.0 85.6 %layer.1 = bf16[384,256]{1,0:T(8,128)(2,1)S(1)} custom-call(bf16[384,256]{1,0:T(8,128)(2,1)} %refs_0_.1, f32[1,2048]{1,0:T(1,128)} %bitcast.12, f32[32,128]{1,0:T(8,128)} %refs_2_.1, f32[32,128]{1,0:T(8,128)} %refs_3_.1, f32[1,128]{1,0:T(1,128)} %bitcast.15, f32[1,128]{1,0:T(1,128)} %bitcast.16, f32[1,128]{1,0:T(1,128)} %bitcast.17, ...), custom_call_target="tpu_custom_call" | custom-call | tf_op jit(solution)/shard_map/layer/pallas_call | solution.py:544
  85.6 0.7 copy.18

commit v5 on v4

--- a/solution.py
+++ b/solution.py
@@ -131,12 +131,15 @@
         first_wait(u, step)
         first_send(u, step)
 
-    SPa, SPb, SCa, SCb, Ua, Ub, D0a, D0b, D1a, D1b = range(10)
+    SPa, SPb, SCa, SCb, Uo, Ua, Ub, D0o, D0a, D0b, D1o, D1a, D1b = range(13)
     SMALL = 4
+    groups = [(u, low, n) for u in (SP, SC) for low, n in ((0, 3), (3, 5))]
+    groups += [(u, low, n) for u in (U, D0, D1) for low, n in ((0, 1), (1, 2), (3, 5))]
 
     def group(g, at, lead=slice(None)):
-        shards_of = pl.ds(0, 3) if g % 2 == 0 else pl.ds(3, 5)
-        return units[g // 2].at[at, shards_of] if g < SMALL else units[g // 2].at[lead, at, shards_of]
+        u, low, n = groups[g]
+        shards_of = pl.ds(low, n)
+        return units[u].at[at, shards_of] if g < SMALL else units[u].at[lead, at, shards_of]
 
     def second_copy(g, way, step):
         at = (q + (step if way else -step) + RING) % RING
@@ -219,7 +222,7 @@
 
         def near(self, way, part):
             rows = pl.ds(part * half, half)
-            return self.copy(self.ring_out.at[1 + way, rows], self.near_in.at[way, rows], 6 + 2 * way + part,
+            return self.copy(self.ring_out.at[1 + way, rows], self.near_in.at[way, rows], 6,
                              tp_of((1, -1)[way], False))
 
         def begin(self, blocks_of):
@@ -228,8 +231,9 @@
                 self.sib_out[k] = across.astype(BF16)
                 self.across(k).start()
                 self.acc[k] = own
-                if k > 0:
-                    self.own(k - 1)
+                if k > 1:
+                    self.own(k - 2)
+            self.own(2)
 
         def own(self, k):
             self.across(k).wait_recv()
@@ -256,9 +260,7 @@
 
         def finish(self):
             self.own(3)
-            for way in range(2):
-                for part in range(2):
-                    self.near(way, part).wait_recv()
+            self.copy(self.near_in, self.near_in, 6, tp_of(1, False)).wait_recv()
             return self.acc[3] + self.near_in[0].astype(F32) + self.near_in[1].astype(F32)
 
         def drain(self):
@@ -301,9 +303,9 @@
 
     value = {}
 
-    def square_copy(d, arriving=False):
-        ref = squares.at[(tp + N_TP - d) % N_TP] if arriving else squares.at[tp]
-        return remote(ref, ref, sq_send.at[0], sq_recv.at[d - 1], fs, (tp + d) % N_TP)
+    def square_copy(d):
+        ref = squares.at[tp]
+        return remote(ref, ref, sq_send.at[0], sq_recv.at[0], fs, (tp + d) % N_TP)
 
     def spatial_branch():
         linear = jnp.dot(normed[...], all_rows(wp, slice(0, 128)), preferred_element_type=F32)
@@ -328,8 +330,8 @@
         value["bias"] = jnp.transpose(jnp.broadcast_to(bias_ref[...], (BLOCK, BLOCK)))
 
     def square_wait():
-        for d in range(1, N_TP):
-            square_copy(d, True).wait_recv()
+        ref = squares.at[0:N_TP - 1]
+        remote(ref, ref, sq_send.at[0], sq_recv.at[0], fs, tp_of(1, False)).wait_recv()
 
     def mix():
         total_sq = squares[0]
@@ -386,13 +388,13 @@
         value["split"] = jnp.dot(value["middle"], value["order"], preferred_element_type=F32)
 
     def down_half(ref):
-        def pair(k, blocks):
-            pieces = [r for zz in blocks for r in plane_rows(ref.at[k], zz, slice(0, 512))]
-            return nt_dot(hidden[:, k * 512:(k + 1) * 512], jnp.concatenate(pieces, axis=0))
-
         def blocks_of(k, dx):
-            blocks = [tp_of(dx, other) for other in (True, False)]
-            both = pair(0, blocks) + pair(1, blocks)
+            rows = [
+                jnp.concatenate(halves, axis=1)
+                for other in (True, False)
+                for halves in zip(*(plane_rows(ref.at[i], tp_of(dx, other), slice(0, 512)) for i in range(2)))
+            ]
+            both = nt_dot(hidden[...], jnp.concatenate(rows, axis=0))
             return both[:, 0:128], both[:, 128:256]
 
         return blocks_of
@@ -411,103 +413,118 @@
         for i in (1, 4, 5, 6, 7, 8, 11, 13):
             fetches[i].wait()
 
-    first_send(D0, 0)
     first_send(D1, 0)
-    small_send(SP)
-    small_send(SC)
     gather1.begin()
     first_send(U, 0)
+    small_send(SP)
+    first_send(D0, 0)
+    small_send(SC)
     first_forward(D1, 1)
-    second_send(D1a)
-    first_forward(D0, 1)
-    second_send(D0a)
-    small_wait(SC, 0)
+    second_send(D0o)
+    first_forward(U, 1)
     small_wait(SP, 0)
     second_send(SPa)
-    small_wait(SP, 1)
+    second_send(Ua)
+    small_wait(SC, 0)
+    second_send(D1o)
     gather1.pass_on()
     second_send(SCa)
+    small_wait(SP, 1)
     second_send(SPb)
-    first_forward(U, 1)
+    first_forward(D0, 1)
+    second_send(D1a)
+    forward(SPa, 1)
     small_wait(SC, 1)
+    second_send(SCb)
+    first_forward(U, 2)
+    forward(Ua, 1)
+    forward(SPb, 1)
+    first_forward(D1, 2)
+    forward(SCa, 1)
+    forward(D1o, 1)
+    second_send(Uo)
+    gather1.far()
     gather1.near()
-    second_send(SCb)
-    second_send(Ua)
-    first_forward(D1, 2)
-    gather1.far()
-    forward(SPa, 1)
-    first_forward(U, 2)
-    forward(SPb, 1)
+    forward(SPa, 2)
+    forward(SCb, 1)
     gather1.wait(0, 1, 2, 3)
-    forward(SCa, 1)
-    forward(SCb, 1)
-    forward(D0a, 1)
+    first_forward(U, 3)
     first_forward(D0, 2)
+    forward(D1a, 1)
+    forward(SPb, 2)
+    forward(SCa, 2)
+    second_send(D0a)
+    forward(Ua, 2)
+    forward(SCb, 2)
+    first_forward(D1, 3)
+    first_wait(U)
+    forward(SPa, 3)
+    first_forward(D0, 3)
+    forward(SPb, 3)
+    forward(D0o, 1)
+    forward(SCa, 3)
+    second_send(Ub)
     late_fetches()
     normalize()
-    forward(SPa, 2)
-    forward(SPb, 2)
-    forward(Ua, 1)
-    first_forward(U, 3)
-    first_forward(D1, 3)
-    first_forward(D0, 3)
-    forward(D1a, 1)
-    forward(SCa, 2)
-    forward(SCb, 2)
-    first_wait(U)
-    forward(SPa, 3)
-    forward(SPb, 3)
-    second_send(Ub)
+    second_wait(SPb)
+    forward(SCb, 3)
     first_wait(D1)
-    forward(SCa, 3)
-    forward(SCb, 3)
+    forward(Uo, 1)
+    second_send(D1b)
+    forward(Ua, 3)
     second_wait(SPa)
-    second_wait(SPb)
-    forward(Ua, 2)
-    forward(D1a, 2)
     spatial_branch()
-    second_send(D1b)
+    forward(D0o, 2)
+    forward(Ub, 1)
     first_wait(D0)
     second_wait(SCa)
+    second_send(D0b)
     second_wait(SCb)
     content_branch()
-    forward(Ub, 1)
+    forward(D0a, 1)
+    forward(D1a, 2)
     square_wait()
-    second_send(D0b)
     mix()
-    forward(D0a, 2)
     scatter1.begin(project_blocks)
+    forward(Uo, 2)
     forward(D1b, 1)
     forward(Ub, 2)
     scatter1.combine()
     forward(D0b, 1)
+    second_wait(Ua)
+    forward(D1o, 2)
     middle()
-    forward(Ua, 3)
+    forward(Uo, 3)
     forward(D1b, 2)
     forward(Ub, 3)
+    forward(D0a, 2)
+    gather2.pass_on()
+    forward(D0b, 2)
+    forward(D1o, 3)
+    gather2.near()
+    forward(D1b, 3)
+    second_wait(Uo)
+    forward(D1a, 3)
+    gather2.wait(0)
+    second_wait(Ub)
+    up_part((0,), True)
+    gather2.far()
     split_middle()
-    gather2.wait(0)
-    gather2.pass_on()
-    gather2.near()
-    forward(D0b, 2)
-    forward(D1b, 3)
-    forward(D1a, 3)
+    forward(D0o, 3)
+    forward(D0a, 3)
     gather2.wait(1, 2)
-    gather2.far()
-    second_wait(Ua)
-    second_wait(Ub)
-    forward(D0a, 3)
-    up_part((0,), True)
     up_part((-1, 1))
     gather2.wait(3)
     forward(D0b, 3)
+    second_wait(D1o)
     up_part((2,))
     second_wait(D1b)
     activate()
     second_wait(D1a)
     scatter3.begin(down_half(wd1))
+    second_wait(D0a)
+    second_wait(D0o)
     second_wait(D0b)
-    second_wait(D0a)
     scatter2.begin(down_half(wd0))
     scatter3.combine()
     scatter2.combine()
@@ -516,7 +533,7 @@
     for u in range(5):
         ref = units[u].at[0, 0:7] if u <= SC else units[u].at[:, 0, 0:7]
         remote(ref, ref, w1_send.at[u], w1_recv.at[u, 0], fs, tp_of(1, False)).wait_send()
-    for g in range(10):
+    for g in range(13):
         ref = group(g, pl.ds(0, 7))
         remote(ref, ref, w2_send.at[g], w2_recv.at[g, 0], fs, tp_of(1, False)).wait_send()
     gather1.drain()
@@ -562,8 +579,8 @@
             vmem((2, rows // 2, 256), BF16), vmem((2, rows, 256), BF16), vmem((4, rows, 256), F32),
             vmem((8, rows, 128), BF16), vmem((8, rows, 128), BF16), vmem((6, rows, 128), BF16),
             vmem((4, rows // 2, 128), BF16), vmem((4, rows, 128), BF16), vmem((8, rows, 128), F32),
-            dma((N_INPUTS,)), dma((5,)), dma((5, HOPS)), dma((10,)), dma((10, HOPS)),
-            dma((2,)), dma((2, 10)), dma((3,)), dma((3, 10)), dma((1,)), dma((7,)),
+            dma((N_INPUTS,)), dma((5,)), dma((5, HOPS)), dma((13,)), dma((13, HOPS)),
+            dma((2,)), dma((2, 10)), dma((3,)), dma((3, 7)), dma((1,)), dma((1,)),
         ],
         compiler_params=pltpu.CompilerParams(
             collective_id=0, has_side_effects=True, vmem_limit_bytes=56 * 1024 * 1024),

time: 86.5 us -> 84.4 us (0.976)
  Pallas kernels: 85.6 us -> 83.5 us
    pallas_call x1, Pallas kernels: 85.6 us -> 83.5 us  [shards(): pl.pallas_call(layer_kernel, out_shape=pltpu.VMEM((rows, width), BF16), i...]
where the time goes in v5:
time: 84.4 us; the launch traced here: 84.2 us
  Pallas kernels  83.5 us (99%)
    pallas_call x1, Pallas kernels, shards(): pl.pallas_call(layer_kernel, out_shape=pltpu.VMEM((rows, width), BF16), i...  83.5 us

profile of v5, /device:TPU:1, one launch (start us, length us, event | category | flops | bytes accessed | tf_op | source)
XLA Modules:
  0.0 84.2 jit_solution(3653766031204167216)
XLA Ops:
  0.0 83.5 %layer.1 = bf16[384,256]{1,0:T(8,128)(2,1)S(1)} custom-call(bf16[384,256]{1,0:T(8,128)(2,1)} %refs_0_.1, f32[1,2048]{1,0:T(1,128)} %bitcast.12, f32[32,128]{1,0:T(8,128)} %refs_2_.1, f32[32,128]{1,0:T(8,128)} %refs_3_.1, f32[1,128]{1,0:T(1,128)} %bitcast.15, f32[1,128]{1,0:T(1,128)} %bitcast.16, f32[1,128]{1,0:T(1,128)} %bitcast.17, ...), custom_call_target="tpu_custom_call" | custom-call | tf_op jit(solution)/shard_map/layer/pallas_call | solution.py:561
  83.5 0.7 copy.18

commit v6 on v5

--- a/solution.py
+++ b/solution.py
@@ -56,7 +56,7 @@
     second_next = (fs_of(p, (q + 1) % RING), fs_of(p, (q + RING - 1) % RING))
 
     barrier = pltpu.get_barrier_semaphore()
-    for to in tuple(fs_of((p + d) % RING, q) for d in range(1, RING)) + second_next:
+    for to in tuple(fs_of(p, (q + d) % RING) for d in range(1, RING)) + first_next:
         pl.semaphore_signal(barrier, inc=1, device_id=(to, tp), device_id_type=MESH)
     for d in range(1, N_TP):
         pl.semaphore_signal(barrier, inc=1, device_id=(fs, (tp + d) % N_TP), device_id_type=MESH)
@@ -81,9 +81,9 @@
 
     for i in (2, 3, 9, 10):
         fetches[i].wait()
-    wp[q, 0] = w_spatial_ref[...].astype(BF16)
-    wc[q, 0, :, 0:128] = w_content_ref[...].astype(BF16)
-    wc[q, 0, :, 128:256] = scaled(w_project_ref[...], project_scale_ref[...])
+    wp[p, 0] = w_spatial_ref[...].astype(BF16)
+    wc[p, 0, :, 0:128] = w_content_ref[...].astype(BF16)
+    wc[p, 0, :, 128:256] = scaled(w_project_ref[...], project_scale_ref[...])
     for i in (0, 12, 14, 15):
         fetches[i].wait()
     tok1[tp] = tokens_ref[...]
@@ -100,7 +100,7 @@
 
     def first_copy(u, src, dst, to, sem, part=None):
         if u <= SC:
-            src_ref, dst_ref = units[u].at[q, src], units[u].at[q, dst]
+            src_ref, dst_ref = units[u].at[p, src], units[u].at[p, dst]
         else:
             lead = slice(None) if part is None else part
             src_ref, dst_ref = units[u].at[lead, q, src], units[u].at[lead, q, dst]
@@ -116,7 +116,7 @@
 
     def small_send(u):
         for d in (1, -1, 2, -2, 3, -3, 4):
-            first_copy(u, 0, places[-d], fs_of((p + d + RING) % RING, q), 0 if abs(d) == 1 else 1).start()
+            first_copy(u, 0, places[-d], fs_of(p, (q + d + RING) % RING), 0 if abs(d) == 1 else 1).start()
 
     def small_wait(u, sem):
         ref = units[u].at[0, 0:2] if sem == 0 else units[u].at[0, 0:5]
@@ -142,11 +142,12 @@
         return units[u].at[at, shards_of] if g < SMALL else units[u].at[lead, at, shards_of]
 
     def second_copy(g, way, step):
-        at = (q + (step if way else -step) + RING) % RING
+        start, to = (p, first_next) if g < SMALL else (q, second_next)
+        at = (start + (step if way else -step) + RING) % RING
         ref = group(g, at)
         if step == HOPS - 1:
             ref = ref.at[:, pl.ds(way * (SLICE // 2), SLICE // 2)] if g < SMALL else group(g, at, way)
-        return remote(ref, ref, w2_send.at[g], w2_recv.at[g, step], second_next[way], tp)
+        return remote(ref, ref, w2_send.at[g], w2_recv.at[g, step], to[way], tp)
 
     def second_send(g, step=0):
         for way in range(2):
@@ -280,17 +281,19 @@
             cols = slice(t * width, (t + 1) * width)
             normed[:, cols] = (tok1[t].astype(F32) * r * mixer_gain_ref[:, cols]).astype(BF16)
 
-    def plane_rows(ref, zz, cols):
+    def plane_rows(ref, zz, cols, small=False):
         rows = []
         for j in range(RING):
-            first, second = jnp.where(core == 0, j, zz), jnp.where(core == 0, zz, j)
-            d = (first - p + RING) % RING
+            straight = 1 if small else 0
+            first = jnp.where(core == straight, j, zz)
+            second = jnp.where(core == straight, zz, j)
+            d = (first - (q if small else p) + RING) % RING
             at = jnp.where((d >= 1) & (d <= HOPS), 2 * d - 1, (2 * (RING - d)) % (2 * RING))
             rows.append(ref[second, at, :, cols])
         return rows
 
     def all_rows(ref, cols):
-        return jnp.concatenate([r for zz in range(RING) for r in plane_rows(ref, zz, cols)], axis=0)
+        return jnp.concatenate([r for zz in range(RING) for r in plane_rows(ref, zz, cols, True)], axis=0)
 
     def set_of(*bufs, low=None):
         return bufs if low is None else tuple(b.at[pl.ds(low * (b.shape[0] // 2), b.shape[0] // 2)] for b in bufs)
@@ -348,7 +351,7 @@
 
     def project_blocks(k, dx):
         return tuple(
-            nt_dot(value["gated"], jnp.concatenate(plane_rows(wc, tp_of(dx, other), slice(128, 256)), axis=0))
+            nt_dot(value["gated"], jnp.concatenate(plane_rows(wc, tp_of(dx, other), slice(128, 256), True), axis=0))
             for other in (True, False))
 
     def middle():
@@ -413,117 +416,117 @@
         for i in (1, 4, 5, 6, 7, 8, 11, 13):
             fetches[i].wait()
 
+    small_send(SP)
+    first_send(U, 0)
+    small_send(SC)
+    second_send(Uo)
+    gather1.begin()
+    second_send(D1o)
+    first_send(D0, 0)
+    second_send(D0o)
     first_send(D1, 0)
-    gather1.begin()
-    first_send(U, 0)
-    small_send(SP)
-    first_send(D0, 0)
-    small_send(SC)
-    first_forward(D1, 1)
-    second_send(D0o)
     first_forward(U, 1)
     small_wait(SP, 0)
+    second_send(Ua)
     second_send(SPa)
-    second_send(Ua)
+    first_forward(D0, 1)
     small_wait(SC, 0)
-    second_send(D1o)
-    gather1.pass_on()
     second_send(SCa)
     small_wait(SP, 1)
     second_send(SPb)
-    first_forward(D0, 1)
-    second_send(D1a)
-    forward(SPa, 1)
+    first_forward(D1, 1)
+    forward(D1o, 1)
     small_wait(SC, 1)
     second_send(SCb)
     first_forward(U, 2)
-    forward(Ua, 1)
+    forward(SPa, 1)
+    second_send(D0a)
+    gather1.pass_on()
+    forward(Uo, 1)
     forward(SPb, 1)
     first_forward(D1, 2)
     forward(SCa, 1)
-    forward(D1o, 1)
-    second_send(Uo)
+    forward(D0o, 1)
+    first_forward(D0, 2)
+    forward(SCb, 1)
+    second_send(D1a)
+    forward(SPa, 2)
+    first_forward(U, 3)
+    forward(SPb, 2)
+    forward(D1o, 2)
+    forward(SCa, 2)
+    first_forward(D0, 3)
+    first_forward(D1, 3)
+    gather1.near()
+    forward(Ua, 1)
+    forward(D1a, 1)
+    forward(SCb, 2)
+    first_wait(U)
     gather1.far()
-    gather1.near()
-    forward(SPa, 2)
-    forward(SCb, 1)
+    forward(SPa, 3)
     gather1.wait(0, 1, 2, 3)
-    first_forward(U, 3)
-    first_forward(D0, 2)
-    forward(D1a, 1)
-    forward(SPb, 2)
-    forward(SCa, 2)
-    second_send(D0a)
-    forward(Ua, 2)
-    forward(SCb, 2)
-    first_forward(D1, 3)
-    first_wait(U)
-    forward(SPa, 3)
-    first_forward(D0, 3)
+    second_send(Ub)
     forward(SPb, 3)
-    forward(D0o, 1)
-    forward(SCa, 3)
-    second_send(Ub)
     late_fetches()
     normalize()
+    first_wait(D1)
+    forward(SCa, 3)
+    forward(D0o, 2)
+    second_send(D1b)
+    forward(SCb, 3)
+    forward(D1o, 3)
+    first_wait(D0)
     second_wait(SPb)
-    forward(SCb, 3)
-    first_wait(D1)
-    forward(Uo, 1)
-    second_send(D1b)
-    forward(Ua, 3)
+    forward(Uo, 2)
+    forward(Ua, 2)
     second_wait(SPa)
     spatial_branch()
-    forward(D0o, 2)
+    forward(D0a, 1)
+    second_wait(SCb)
     forward(Ub, 1)
-    first_wait(D0)
     second_wait(SCa)
+    content_branch()
     second_send(D0b)
-    second_wait(SCb)
-    content_branch()
-    forward(D0a, 1)
+    square_wait()
     forward(D1a, 2)
-    square_wait()
     mix()
     scatter1.begin(project_blocks)
-    forward(Uo, 2)
     forward(D1b, 1)
+    forward(Uo, 3)
+    scatter1.combine()
     forward(Ub, 2)
-    scatter1.combine()
     forward(D0b, 1)
-    second_wait(Ua)
-    forward(D1o, 2)
+    forward(Ua, 3)
     middle()
-    forward(Uo, 3)
     forward(D1b, 2)
     forward(Ub, 3)
+    second_wait(Uo)
     forward(D0a, 2)
     gather2.pass_on()
+    gather2.wait(0)
     forward(D0b, 2)
-    forward(D1o, 3)
+    forward(D0o, 3)
+    split_middle()
+    forward(D1a, 3)
     gather2.near()
     forward(D1b, 3)
-    second_wait(Uo)
-    forward(D1a, 3)
-    gather2.wait(0)
     second_wait(Ub)
+    gather2.wait(1, 2)
+    second_wait(Ua)
     up_part((0,), True)
+    forward(D0a, 3)
     gather2.far()
-    split_middle()
-    forward(D0o, 3)
-    forward(D0a, 3)
-    gather2.wait(1, 2)
     up_part((-1, 1))
     gather2.wait(3)
     forward(D0b, 3)
+    up_part((2,))
+    second_wait(D0o)
+    activate()
+    second_wait(D1b)
+    second_wait(D1a)
     second_wait(D1o)
-    up_part((2,))
-    second_wait(D1b)
-    activate()
-    second_wait(D1a)
     scatter3.begin(down_half(wd1))
     second_wait(D0a)
-    second_wait(D0o)
     second_wait(D0b)
     scatter2.begin(down_half(wd0))
     scatter3.combine()

time: 84.4 us -> 83.6 us (level)
  no operation moved by 1% of the time
where the time goes in v6:
time: 83.6 us; the launch traced here: 83.5 us
  Pallas kernels  82.8 us (99%)
    pallas_call x1, Pallas kernels, shards(): pl.pallas_call(layer_kernel, out_shape=pltpu.VMEM((rows, width), BF16), i...  82.8 us

profile of v6, /device:TPU:1, one launch (start us, length us, event | category | flops | bytes accessed | tf_op | source)
XLA Modules:
  0.0 83.5 jit_solution(14247252111716379987)
XLA Ops:
  0.0 82.8 %layer.1 = bf16[384,256]{1,0:T(8,128)(2,1)S(1)} custom-call(bf16[384,256]{1,0:T(8,128)(2,1)} %refs_0_.1, f32[1,2048]{1,0:T(1,128)} %bitcast.12, f32[32,128]{1,0:T(8,128)} %refs_2_.1, f32[32,128]{1,0:T(8,128)} %refs_3_.1, f32[1,128]{1,0:T(1,128)} %bitcast.15, f32[1,128]{1,0:T(1,128)} %bitcast.16, f32[1,128]{1,0:T(1,128)} %bitcast.17, ...), custom_call_target="tpu_custom_call" | custom-call | tf_op jit(solution)/shard_map/layer/pallas_call | solution.py:564
  82.8 0.7 copy.18

commit v7 on v6

--- a/solution.py
+++ b/solution.py
@@ -359,7 +359,7 @@
         tok2[tp] = value["middle"]
         gather2.begin()
 
-    def up_part(dxs, first=False):
+    def up_part(dxs, first=False, last=False):
         blocks = [tp_of(dx, other) for dx in dxs for other in (False, True)]
         terms = []
         for t in blocks:
@@ -369,18 +369,19 @@
             gain = channel_gain_ref[:, pl.ds(pl.multiple_of(t * width, 128), width)]
             terms.append((v * gain).astype(BF16))
         left = jnp.concatenate(terms, axis=1)
+        if last:
+            r = lax.rsqrt(value["sum"] / (N_TP * width) + EPSILON)
         for k in range(2):
             for low in range(0, 512, 256):
                 cols = slice(low, low + 256)
                 right = jnp.concatenate([r for t in blocks for r in plane_rows(wu.at[k], t, cols)], axis=0)
                 at = slice(k * 512 + low, k * 512 + low + 256)
                 part = jnp.dot(left, right, preferred_element_type=F32)
-                up_acc[:, at] = part if first else up_acc[:, at] + part
-
-    def activate():
-        r = lax.rsqrt(value["sum"] / (N_TP * width) + EPSILON)
-        up = jnp.maximum(up_acc[...] * r * up_scale_ref[...], 0.0)
-        hidden[...] = (up * up).astype(BF16)
+                if last:
+                    up = jnp.maximum((up_acc[:, at] + part) * r * up_scale_ref[:, at], 0.0)
+                    hidden[:, at] = (up * up).astype(BF16)
+                else:
+                    up_acc[:, at] = part if first else up_acc[:, at] + part
 
     def split_middle():
         natural = lax.broadcasted_iota(jnp.int32, (width, width), 0)
@@ -519,9 +520,8 @@
     up_part((-1, 1))
     gather2.wait(3)
     forward(D0b, 3)
-    up_part((2,))
+    up_part((2,), last=True)
     second_wait(D0o)
-    activate()
     second_wait(D1b)
     second_wait(D1a)
     second_wait(D1o)

time: 83.6 us -> 83.6 us (level)
  no operation moved by 1% of the time
where the time goes in v7:
time: 83.6 us; the launch traced here: 83.5 us
  Pallas kernels  82.8 us (99%)
    pallas_call x1, Pallas kernels, shards(): pl.pallas_call(layer_kernel, out_shape=pltpu.VMEM((rows, width), BF16), i...  82.8 us

profile of v7, /device:TPU:1, one launch (start us, length us, event | category | flops | bytes accessed | tf_op | source)
XLA Modules:
  0.0 83.5 jit_solution(7455226238986981657)
XLA Ops:
  0.0 82.8 %layer.1 = bf16[384,256]{1,0:T(8,128)(2,1)S(1)} custom-call(bf16[384,256]{1,0:T(8,128)(2,1)} %refs_0_.1, f32[1,2048]{1,0:T(1,128)} %bitcast.12, f32[32,128]{1,0:T(8,128)} %refs_2_.1, f32[32,128]{1,0:T(8,128)} %refs_3_.1, f32[1,128]{1,0:T(1,128)} %bitcast.15, f32[1,128]{1,0:T(1,128)} %bitcast.16, f32[1,128]{1,0:T(1,128)} %bitcast.17, ...), custom_call_target="tpu_custom_call" | custom-call | tf_op jit(solution)/shard_map/layer/pallas_call | solution.py:564
  82.8 0.7 copy.18
